TPU v7x, 32 devices: a whole 2x2x4 slice. The times are simulated.
32 devices in a mesh: rep: 2 (over x), fs: 8 (over z, y), tp: 2 (over core).
Axes of the slice: x: 2, y: 2, z: 4, core: 2. Of those that a mesh axis runs over, the one named last changes fastest.
Arguments:
- tokens: bfloat16 [4096, 2048], P(('rep', 'fs')), may hold values from -6 to 6
- first_gain: float32 [2048], replicated, may hold values from 0.1 to 1.9
- value_weight: float32 [2048, 1024], P('fs', 'tp'), may hold values from -0.125 to 0.125
- gate_weight: float32 [2048, 1024], P('fs', 'tp'), may hold values from -0.125 to 0.125
- value_scale: float32 [1024], P('tp'), may hold values from 0.5 to 2
- gate_scale: float32 [1024], P('tp'), may hold values from 0.5 to 2
- conv_taps: float32 [31, 1024], P(None, 'tp'), may hold values from -7 to 7
- chan_gain: float32 [1024], P('tp'), may hold values from 0.1 to 1.9
- mixout_weight: float32 [1024, 2048], P('tp', 'fs'), may hold values from -0.1875 to 0.1875
- mixout_scale: float32 [2048], P('fs'), may hold values from 0.5 to 2
- second_gain: float32 [2048], replicated, may hold values from 0.1 to 1.9
- up_weight: float32 [2048, 8192], P('fs', 'tp'), may hold values from -0.125 to 0.125
- up_scale: float32 [8192], P('tp'), may hold values from 0.5 to 2
- down_weight: float32 [8192, 2048], P('tp', 'fs'), may hold values from -0.0625 to 0.0625
- down_scale: float32 [2048], P('fs'), may hold values from 0.5 to 2
Outputs:
- layer_out: bfloat16 [4096, 2048], P(('rep', 'fs'))
All inputs are finite; a program needn't handle non-finite values.
Results may differ from a plain program's by a relative error of at most 0.025.
Values may be sent and summed in bfloat16 or wider, within the bound.
No kernel may reach another device: no remote copies, remote signals or barrier semaphores. Data moves between devices by JAX's collectives and lax.ppermute only.
A program may use at most 128 MiB of HBM per device.

v0:
```python
import functools

import jax
import jax.numpy as jnp
from jax import lax
from jax.experimental import pallas as pl
from jax.experimental.pallas import tpu as pltpu
from jax.sharding import PartitionSpec as P


SEQ_LEN = 128
EPS = 1e-05
PAD = 16


ANY = pl.BlockSpec(memory_space=pl.ANY)
SMEM = pl.BlockSpec(memory_space=pltpu.SMEM)
VMEM = pl.BlockSpec(memory_space=pltpu.VMEM)
BF16 = jnp.bfloat16
F32 = jnp.float32


def rms_rows(rows, gain):
    values = rows.astype(F32)
    scaled = values * lax.rsqrt(jnp.mean(values * values, axis=-1, keepdims=True) + EPS)
    return (scaled * gain).astype(BF16)


def start_all(pairs, sems):
    copies = [pltpu.make_async_copy(s, d, sems.at[i]) for i, (s, d) in enumerate(pairs)]
    for c in copies:
        c.start()
    return copies


def lanes(ref, index, width):
    if ref.shape[1] == width:
        return slice(None)
    return pl.ds(pl.multiple_of(index * width, width), width)


def wait_all(copies):
    for c in copies:
        c.wait()


def glu_conv_kernel(places, offsets, rows, n_own, pos, vs, gs, taps, *refs):
    nb, n_parts = len(places), len(offsets)
    own = refs[0]
    parts = refs[1 : 1 + n_parts]
    blocks = refs[1 + n_parts : 1 + n_parts + nb]
    conv_out, stat_out, x, w, padded, sems = refs[1 + n_parts + nb :]
    n = parts[0].shape[0]
    pairs = [(own, x.at[pl.ds(0, n_own)])]
    for p in range(n_parts):
        pairs.append((parts[p], x.at[pl.ds(pl.multiple_of(offsets[p](pos), n), n)]))
    for b in range(nb):
        pairs.append((blocks[b], w.at[pl.ds(pl.multiple_of(places[b](pos) * rows, rows), rows)]))
    wait_all(start_all(pairs, sems))
    total, width = conv_out.shape
    chan = lanes(vs, pos[0], width)
    vs_own = vs[:, chan].astype(BF16).astype(F32)
    gs_own = gs[:, chan].astype(BF16).astype(F32)
    n_seq = total // SEQ_LEN
    k = taps.shape[0]
    lead = padded.shape[1] - SEQ_LEN
    both = jnp.dot(x[...], w[...], preferred_element_type=F32)
    glu = both[:, :width] * vs_own * jax.nn.sigmoid(both[:, width:] * gs_own)
    for s in range(n_seq):
        padded[s, :lead, :] = jnp.zeros((lead, width), F32)
        padded[s, lead:, :] = glu[s * SEQ_LEN : (s + 1) * SEQ_LEN, :]
    for s in range(n_seq):
        at = s * SEQ_LEN
        acc = jnp.zeros((SEQ_LEN, width), F32)
        for j in range(k):
            start = lead - (k - 1) + j
            acc = acc + taps[j : j + 1, chan] * padded[s, start : start + SEQ_LEN, :]
        conv_out[at : at + SEQ_LEN, :] = acc
    conv = conv_out[...]
    sums = jnp.sum(conv, axis=1, keepdims=True)
    squares = jnp.sum(conv * conv, axis=1, keepdims=True)
    lane = lax.broadcasted_iota(jnp.int32, (total, 128), 1)
    stat_out[...] = jnp.where(lane == 0, sums, squares).T[:8, :]


def mix_kernel(places, turns, reps, tps, n, channels, pos, gain, conv, *refs):
    nb, n_stats = len(places), len(turns)
    stats = refs[:n_stats]
    blocks = refs[n_stats : n_stats + nb]
    outs = refs[n_stats + nb : n_stats + nb + tps]
    w, columns, sems = refs[n_stats + nb + tps :]
    cols = blocks[0].shape[1]
    copies = start_all(
        [(blocks[b], w.at[:, pl.ds(pl.multiple_of(places[b](pos) * cols, cols), cols)]) for b in range(nb)],
        sems,
    )
    width = conv.shape[1]
    stat = stats[0][...]
    per = n * tps
    for s, turn in zip(stats[1:], turns[1:]):
        blocks_of = [(q - turn) % reps for q in range(reps)]
        stat = stat + jnp.concatenate([s[:, q * per : (q + 1) * per] for q in blocks_of], axis=1)
    columns[...] = stat.T
    own_gain = gain[:, lanes(gain, pos[0], width)]
    wait_all(copies)
    scale = w[width : width + 1, :].astype(F32)
    mixed = []
    for k in range(tps):
        for r in range(reps):
            at = pl.multiple_of(r * per + lax.rem(pos[3] + tps - k, tps) * n, n)
            column = columns[pl.ds(at, n), :]
            mean = column[:, 0:1] / channels
            var = column[:, 1:2] / channels - mean * mean
            v = (conv[pl.ds(at, n), :] - mean) * lax.rsqrt(var + EPS) * own_gain
            mixed.append((v / (1.0 + jnp.exp(-v))).astype(BF16))
    mixed = jnp.concatenate(mixed, axis=0)
    term = (jnp.dot(mixed, w[:width, :], preferred_element_type=F32) * scale).astype(BF16)
    for k in range(tps):
        outs[k][...] = term[k * reps * n : (k + 1) * reps * n, :]


def up_kernel(places, n_tok, tps, pos, *refs):
    nb = len(places)
    scales = refs[:tps]
    refs = refs[tps:]
    toks = refs[:n_tok]
    ups = refs[n_tok : n_tok + tps * nb]
    out, x, wu, stage, sems, out_sems = refs[n_tok + tps * nb :]
    units = wu.shape[1] // tps
    rows = ups[0].shape[0]
    n = toks[0].shape[0]
    pairs = [(t, x.at[pl.ds(i * n, n)]) for i, t in enumerate(toks)]
    for k in range(tps):
        for b in range(nb):
            at = pl.ds(pl.multiple_of(places[b](pos) * rows, rows), rows)
            pairs.append((ups[k * nb + b], wu.at[at, pl.ds(k * units, units)]))
    copies = start_all(pairs, sems)
    wait_all(copies[:n_tok])
    step = min(x.shape[0], 512)
    writes = []
    for k in range(tps):
        wait_all(copies[n_tok + k * nb : n_tok + (k + 1) * nb])
        for at in range(0, x.shape[0], step):
            w = wu[:, k * units : (k + 1) * units]
            up = jnp.dot(x[at : at + step, :], w, preferred_element_type=F32) * scales[k][...].astype(BF16).astype(F32)
            stage[at : at + step, k * units : (k + 1) * units] = jnp.square(jnp.maximum(up, 0.0)).astype(BF16)
        cut = pl.ds(k * units, units)
        writes.append(pltpu.make_async_copy(stage.at[:, cut], out.at[:, cut], out_sems.at[k]))
        writes[-1].start()
    wait_all(writes)


def down_kernel(places, tps, order, n, kept_rows, pos, hidden, *refs):
    nd = len(places)
    downs = refs[: tps * nd]
    kept, sent, h, wd, ws, sems = refs[tps * nd :]
    cols = downs[0].shape[1]
    units = h.shape[1] // tps
    pairs = [(hidden, h)]
    for b in range(nd):
        at = pl.ds(pl.multiple_of(places[b](pos) * cols, cols), cols)
        for k in range(tps):
            pairs.append((downs[k * nd + b].at[pl.ds(0, units)], wd.at[pl.ds(k * units, units), at]))
        pairs.append((downs[b].at[pl.ds(units, PAD)], ws.at[:, at]))
    wait_all(start_all(pairs, sems))
    scale = ws[0:1, :].astype(F32)
    term = jnp.dot(h[...], wd[...], preferred_element_type=F32) * scale
    for j, to in enumerate(order):
        rows = term[j * n : (j + 1) * n, :]
        if to * n < kept_rows:
            kept[to * n : (to + 1) * n, :] = rows
        else:
            sent[to * n - kept_rows : (to + 1) * n - kept_rows, :] = rows.astype(BF16)


def final_kernel(inner, pair, cols, tps, pos, *refs):
    out = refs[-1]
    n_parts = 1 + inner
    base = pos[1] - lax.rem(pos[1], pair)
    for c in range(tps):
        parts = refs[c * n_parts : (c + 1) * n_parts]
        n = parts[0].shape[0]
        rows = pl.ds(pl.multiple_of(lax.rem(pos[3] + tps - c, tps) * n, n), n)
        wide = parts[0].shape[1]
        out[rows, pl.ds(pl.multiple_of(base * inner * cols, cols), wide)] = parts[0][...]
        for k in range(inner):
            for z in range(pair):
                block = (pair - base + z) * inner + lax.rem(pos[2] + inner - k, inner)
                at = pl.multiple_of(block * cols, cols)
                out[rows, pl.ds(at, cols)] = parts[1 + k][:, z * cols : (z + 1) * cols]


def shift(array, axis, by):
    size = lax.axis_size(axis)
    return lax.ppermute(array, axis, [(i, (i + by) % size) for i in range(size)])


def on_device(
    tokens,
    first_gain,
    value_weight,
    gate_weight,
    value_scale,
    gate_scale,
    conv_taps,
    chan_gain,
    mixout_weight,
    mixout_scale,
    second_gain,
    up_weight,
    up_scale,
    down_weight,
    down_scale,
):
    reps, fss, tps = lax.axis_size("rep"), lax.axis_size("fs"), lax.axis_size("tp")
    outer, pair = 4, 2
    inner = fss // outer
    xi, fi, ci = lax.axis_index("rep"), lax.axis_index("fs"), lax.axis_index("tp")
    zi, yi = fi // inner, fi % inner
    count, width = tokens.shape
    n = count // tps

    def along(a, to):
        return lax.ppermute(a, "fs", [(o * inner + i, to(o, i)) for o in range(outer) for i in range(inner)])

    def z_swap(a, m):
        return along(a, lambda o, i: (o ^ m) * inner + i)

    def y_shift(a, s):
        return along(a, lambda o, i: o * inner + (i + s) % inner)

    def pair_shift(a, s):
        return along(a, lambda o, i: (o // pair * pair + (o + s) % pair) * inner + i)

    pos = jnp.stack([xi, zi, yi, ci]).astype(jnp.int32)

    def spread(got):
        if inner <= 2:
            return [list(got.values())] + [[y_shift(b, k) for b in got.values()] for k in range(1, inner)]
        stack = jnp.stack(list(got.values()))
        moved = [y_shift(stack, k) for k in range(1, inner)]
        return [list(got.values())] + [[m[s] for s in range(outer)] for m in moved]

    def gather(block):
        got = {"0": block, "a": z_swap(block, 1), "b": z_swap(block, 2)}
        got["c"] = z_swap(got["b"], 1)
        return spread(got)

    def exchange(blocks):
        got = {"0": blocks[0]}
        for m in range(1, outer):
            got[str(m)] = z_swap(blocks[m % pair], m)
        return spread(got)

    def place(m, k):
        return lambda p: (p[1] ^ m) * inner + lax.rem(p[2] + inner - k, inner)

    all_places = [place(m, k) for k in range(inner) for m in range(outer)]

    def flat(blocks):
        return [b for row in blocks for b in row]

    def take(a, at, size, axis):
        return lax.dynamic_slice_in_dim(a, at * size, size, axis=axis)

    mine = value_weight.shape[1] // reps
    vg = jnp.concatenate(
        [take(value_weight, xi, mine, 1).astype(BF16), take(gate_weight, xi, mine, 1).astype(BF16)], axis=1
    )

    def channels_of(a):
        return a if mine % 128 == 0 else take(a, xi, mine, 1)

    vg_blocks = flat(gather(vg))

    def with_scale(block, scale):
        rows = jnp.broadcast_to(scale.astype(BF16)[None, :], (PAD, scale.shape[0]))
        return jnp.concatenate([block.astype(BF16), rows], axis=0)

    def columns(blocks, at):
        cols = blocks[0].shape[1]
        if cols % 128 == 0:
            return blocks, at
        joined = jnp.zeros((blocks[0].shape[0], cols * len(blocks)), BF16)
        for block, spot in zip(blocks, at):
            joined = lax.dynamic_update_slice_in_dim(joined, block, spot(pos) * cols, axis=1)
        return [joined], [lambda p: 0]

    mix_own = with_scale(take(mixout_weight, xi, mine, 0), mixout_scale)
    mix_blocks, mix_places = columns(flat(gather(mix_own)), all_places)

    normed = rms_rows(tokens, first_gain)
    half = take(normed, ci, n, 0)
    parts, offsets = [], []
    for r in range(1, reps):
        moved = shift(half, "rep", r)
        for k in range(tps):
            parts.append(shift(moved, "tp", k) if k else moved)
            offsets.append(lambda p, r=r, k=k: r * count + lax.rem(p[3] + tps - k, tps) * n)

    groups = reps * pair
    units = up_weight.shape[1] // groups

    at_pair = [xi * pair + (zi + s) % pair for s in range(pair)]
    ups = [take(up_weight, g, units, 1).astype(BF16) for g in at_pair]
    downs = [with_scale(take(down_weight, g, units, 0), down_scale) for g in at_pair]

    def share(parts):
        if tps == 2:
            return [[blocks, [shift(b, "tp", 1) for b in blocks]] for blocks in parts]
        shared = []
        for blocks in parts:
            stack = jnp.stack(blocks)
            moved = [shift(stack, "tp", k) for k in range(1, tps)]
            shared.append([blocks] + [[m[s] for s in range(len(blocks))] for m in moved])
        return shared

    up_blocks = exchange(ups)
    up_blocks = share(up_blocks)
    up_blocks = [b for k in range(tps) for part in up_blocks for b in part[k]]
    down_blocks = exchange(downs)
    down_blocks = share(down_blocks)
    own_scale = take(up_scale, at_pair[0], units, 0)[None, :]
    up_scales = [own_scale] + [shift(own_scale, "tp", k) for k in range(1, tps)]

    total = reps * count
    rows = value_weight.shape[0]
    depth = rows * fss
    lead = -(-(conv_taps.shape[0] - 1) // 8) * 8
    conv, stat = pl.pallas_call(
        functools.partial(glu_conv_kernel, all_places, offsets, rows, count),
        out_shape=(
            jax.ShapeDtypeStruct((total, mine), F32),
            jax.ShapeDtypeStruct((8, total), F32),
        ),
        in_specs=[SMEM, VMEM, VMEM, VMEM] + [ANY] * (1 + len(parts) + fss),
        out_specs=(VMEM, VMEM),
        scratch_shapes=[
            pltpu.VMEM((total, width), BF16),
            pltpu.VMEM((depth, 2 * mine), BF16),
            pltpu.VMEM((total // SEQ_LEN, SEQ_LEN + lead, mine), F32),
            pltpu.SemaphoreType.DMA((1 + len(parts) + fss,)),
        ],
        name="glu_conv",
    )(pos, channels_of(value_scale[None, :]), channels_of(gate_scale[None, :]), channels_of(conv_taps), normed, *parts, *vg_blocks)

    stats = [stat]
    for r in range(reps):
        for k in range(tps):
            if r or k:
                to = [
                    (i * tps + j, (i + r) % reps * tps + (j + k) % tps)
                    for i in range(reps)
                    for j in range(tps)
                ]
                stats.append((r, lax.ppermute(stat, ("rep", "tp"), to)))
    turns = [0] + [r for r, _ in stats[1:]]
    aligned = [stat] + [t for _, t in stats[1:]]
    n_mix = len(mix_blocks)
    mix_terms = pl.pallas_call(
        functools.partial(mix_kernel, mix_places, turns, reps, tps, n, float(mine * reps * tps)),
        out_shape=tuple(jax.ShapeDtypeStruct((reps * n, width), BF16) for _ in range(tps)),
        in_specs=[SMEM, VMEM, VMEM] + [VMEM] * len(aligned) + [ANY] * n_mix,
        out_specs=tuple(VMEM for _ in range(tps)),
        scratch_shapes=[
            pltpu.VMEM((mine + PAD, width), BF16),
            pltpu.VMEM((total, 8), F32),
            pltpu.SemaphoreType.DMA((n_mix,)),
        ],
        name="mix",
    )(pos, channels_of(chan_gain[None, :]), conv, *aligned, *mix_blocks)
    mix_got = [mix_terms[0]] + [shift(mix_terms[k], "tp", -k) for k in range(1, tps)]

    def added(terms, at, size):
        total = terms[0][at : at + size].astype(F32)
        for t in terms[1:]:
            total = total + t[at : at + size].astype(F32)
        return total

    sent = [shift(added(mix_got, r * n, n).astype(BF16), "rep", -r) for r in range(1, reps)]
    mix_sum = added(mix_got, 0, n)
    for t in sent:
        mix_sum = mix_sum + t.astype(F32)
    middle = (take(tokens, ci, n, 0).astype(F32) + mix_sum).astype(BF16)
    normed2 = rms_rows(middle, second_gain)

    across = [normed2] + [shift(normed2, "rep", r) for r in range(1, reps)]
    beside = [normed2] + [pair_shift(normed2, q) for q in range(1, pair)]
    local = {(0, r): [across[r]] for r in range(reps)}
    for q in range(1, pair):
        local[q, 0] = [beside[q]]
        for r in range(1, reps):
            local[q, r] = [shift(beside[q], "rep", r)]
    cells = [(q, r) for q in range(pair) for r in range(reps)]
    toks = [t for cell in cells for t in local[cell]]
    hidden = pl.pallas_call(
        functools.partial(up_kernel, all_places, len(toks), tps),
        out_shape=jax.ShapeDtypeStruct((len(cells) * n, tps * units), BF16),
        in_specs=[SMEM] + [VMEM] * tps + [ANY] * (len(toks) + tps * fss),
        out_specs=ANY,
        scratch_shapes=[
            pltpu.VMEM((len(cells) * n, width), BF16),
            pltpu.VMEM((depth, tps * units), BF16),
            pltpu.VMEM((len(cells) * n, tps * units), BF16),
            pltpu.SemaphoreType.DMA((len(toks) + tps * fss,)),
            pltpu.SemaphoreType.DMA((tps,)),
        ],
        name="up",
    )(pos, *up_scales, *toks, *up_blocks)

    per = len(cells) * n
    block_cols = width // fss
    own_pair = [
        (k, m, lambda p, m=m, k=k: (p[1] ^ m) % pair * inner + lax.rem(p[2] + inner - k, inner))
        for k in range(inner)
        for m in range(pair)
    ]
    other = [[(k, m, lambda p, m=m: (p[1] ^ m) % pair) for m in range(pair, outer)] for k in range(inner)]
    base = zi // pair * pair
    starts = [[(base * inner) * block_cols]] + [
        [((pair - base + z) * inner + (yi - k) % inner) * block_cols for z in range(pair)] for k in range(inner)
    ]
    results = []
    for part, members in enumerate([own_pair] + other):
        blocks = []
        for h in range(tps):
            cut, at = columns([down_blocks[k][h][m] for k, m, _ in members], [f for _, _, f in members])
            blocks += cut
        n_cols = len(members) * block_cols
        rep_first = part % 2 == 0
        first, second = (reps, pair) if rep_first else (pair, reps)
        size = second * n
        order = tuple(r * pair + q if rep_first else q * reps + r for q, r in cells)
        kept, sent = pl.pallas_call(
            functools.partial(down_kernel, at, tps, order, n, size),
            out_shape=(
                jax.ShapeDtypeStruct((size, n_cols), F32),
                jax.ShapeDtypeStruct((per - size, n_cols), BF16),
            ),
            in_specs=[SMEM, ANY] + [ANY] * len(blocks),
            out_specs=(VMEM, VMEM),
            scratch_shapes=[
                pltpu.VMEM((per, tps * units), BF16),
                pltpu.VMEM((tps * units, n_cols), BF16),
                pltpu.VMEM((PAD, n_cols), BF16),
                pltpu.SemaphoreType.DMA((1 + len(at) * (tps + 1),)),
            ],
        )(pos, hidden, *blocks)

        def over_rep(a, j):
            return shift(a.astype(BF16), "rep", -j)

        def over_pair(a, j):
            return pair_shift(a.astype(BF16), -j)

        send_first, send_second = (over_rep, over_pair) if rep_first else (over_pair, over_rep)
        moved = [send_first(sent[(j - 1) * size : j * size], j) for j in range(1, first)]

        def after_first(j):
            total = kept[j * n : (j + 1) * n]
            for t in moved:
                total = total + t[j * n : (j + 1) * n].astype(F32)
            return total

        ready = [after_first(j).astype(BF16) for j in range(1, second)]
        last = [send_second(a, j) for j, a in enumerate(ready, 1)]
        total = after_first(0)
        for t in last:
            total = total + t.astype(F32)
        wide = n_cols // len(starts[part])
        own_middle = [lax.dynamic_slice_in_dim(middle, start, wide, axis=1) for start in starts[part]]
        results.append((jnp.concatenate(own_middle, axis=1).astype(F32) + total).astype(BF16))

    pieces = [[shift(a, "tp", c) if c else a for a in results] for c in range(tps)]
    if block_cols % 128 == 0:
        return pl.pallas_call(
            functools.partial(final_kernel, inner, pair, block_cols, tps),
            out_shape=jax.ShapeDtypeStruct((count, width), BF16),
            in_specs=[SMEM] + [VMEM] * (len(results) * tps),
            out_specs=VMEM,
            name="final",
        )(pos, *[a for row in pieces for a in row])
    result = jnp.zeros((count, width), BF16)
    for c in range(tps):
        for part, piece in enumerate(pieces[c]):
            wide = piece.shape[1] // len(starts[part])
            for j, start in enumerate(starts[part]):
                cut = piece[:, j * wide : (j + 1) * wide]
                result = lax.dynamic_update_slice(result, cut, ((ci - c) % tps * n, start))
    return result


def solution(mesh):
    placed = (
        P(("rep", "fs"), None),
        P(),
        P("fs", "tp"),
        P("fs", "tp"),
        P("tp"),
        P("tp"),
        P(None, "tp"),
        P("tp"),
        P("tp", "fs"),
        P("fs"),
        P(),
        P("fs", "tp"),
        P("tp"),
        P("tp", "fs"),
        P("fs"),
    )

    return jax.shard_map(on_device, mesh=mesh, in_specs=placed, out_specs=P(("rep", "fs"), None), check_vma=False)
```

profile of v0, /device:TPU:0, one launch (start us, length us, event | category | flops | bytes accessed | tf_op | source)
XLA Modules:
  0.0 313.0 jit_solution(13547253133051693465)
XLA Ops:
  0.0 1.6 fusion
  1.6 1.5 fusion.2.refs_0_
  3.2 3.0 collective-permute-start
  6.2 1.2 dynamic-slice_convert_fusion.5
  7.4 2.7 collective-permute-start.3
  10.6 1.6 collective-permute-start.2
  12.6 15.4 %collective-permute-done.13.refs_6_ = bf16[272,256]{1,0:T(8,128)(2,1)} collective-permute-done((bf16[272,256]{1,0:T(8,128)(2,1)S(1)}, bf16[272,256]{1,0:T(8,128)(2,1)}, u32[]{:S(2)}, u32[]{:S(2)}) %collective-permute-start.13) | collective-permute-done | bytes 139296 | tf_op jit(solution)/shard_map/ppermute | solution.py:224
  28.0 1.5 collective-permute-start.5
  30.6 1.5 collective-permute-start.14
  32.1 5.0 %collective-permute-done.5.refs_7_ = bf16[256,512]{1,0:T(8,128)(2,1)S(1)} collective-permute-done((bf16[256,512]{1,0:T(8,128)(2,1)S(1)}, bf16[256,512]{1,0:T(8,128)(2,1)S(1)}, u32[]{:S(2)}, u32[]{:S(2)}) %collective-permute-start.5) | collective-permute-done | bytes 262176 | tf_op jit(solution)/shard_map/ppermute | solution.py:224
  37.1 1.5 collective-permute-start.6
  39.4 1.3 collective-permute-start.15
  40.7 2.0 collective-permute-done.7.refs_9_
  42.8 0.7 copy-done.49
  43.5 1.5 collective-permute-start.17
  45.6 2.8 collective-permute-done.6.refs_8_
  48.5 1.5 collective-permute-start.16
  50.0 4.1 %collective-permute-done.8.refs_10_ = bf16[256,512]{1,0:T(8,128)(2,1)} collective-permute-done((bf16[256,512]{1,0:T(8,128)(2,1)}, bf16[256,512]{1,0:T(8,128)(2,1)}, u32[]{:S(2)}, u32[]{:S(2)}) %collective-permute-start.8) | collective-permute-done | bytes 262176 | tf_op jit(solution)/shard_map/ppermute | solution.py:224
  54.1 1.5 collective-permute-start.18
  55.7 0.8 copy-done.42
  56.4 7.7 %glu_conv.1 = (f32[512,256]{1,0:T(8,128)}, f32[8,512]{1,0:T(8,128)}) custom-call(s32[4]{0:T(128)} %pad_add_fusion.pos, f32[1,512]{1,0:T(1,128)} %bitcast.10, f32[1,512]{1,0:T(1,128)} %bitcast.11, f32[31,512]{1,0:T(8,128)} %taps.1, bf16[256,2048]{1,0:T(8,128)(2,1)} %copy-done.2, bf16[128,2048]{1,0:T(8,128)(2,1)} %copy-done.41, bf16[128,2048]{1,0:T(8,128)(2,1)} %copy-done.42, ...), custom_call_target="tpu_custom_call" | custom-call | tf_op jit(solution)/shard_map/glu_conv/pallas_call | solution.py:330
  64.7 1.7 collective-permute-start.9
  66.4 1.7 dynamic-slice_convert_fusion.2
  69.3 4.7 %mix.1 = (bf16[256,2048]{1,0:T(8,128)(2,1)}, bf16[256,2048]{1,0:T(8,128)(2,1)}) custom-call(s32[4]{0:T(128)} %pad_add_fusion.pos, f32[1,512]{1,0:T(1,128)} %bitcast.12, f32[512,256]{1,0:T(8,128)} %get-tuple-element.15.conv, f32[8,512]{1,0:T(8,128)} %get-tuple-element.16.refs_0_, f32[8,512]{1,0:T(8,128)} %copy-done.55, f32[8,512]{1,0:T(8,128)} %copy-done.53, ...), custom_call_target="tpu_custom_call" | custom-call | tf_op jit(solution)/shard_map/mix/pallas_call | solution.py:360
  74.1 0.7 dynamic_slice.51
  75.3 3.5 %collective-permute-start.26 = (bf16[256,1024]{1,0:T(8,128)(2,1)S(1)}, bf16[256,1024]{1,0:T(8,128)(2,1)S(1)}, u32[]{:S(2)}, u32[]{:S(2)}) collective-permute-start(bf16[256,1024]{1,0:T(8,128)(2,1)S(1)} %get-tuple-element.30.refs_6_), channel_id=1, source_target_pairs={{0,8},{2,10},{4,12},{6,14},{8,0},{10,2},{12,4},{14,6},{1,9},{3,11}... | collective-permute-start | bytes 1572872 | tf_op jit(solution)/shard_map/ppermute | solution.py:224
  79.7 6.4 %collective-permute-done.25.refs_7_ = bf16[256,1024]{1,0:T(8,128)(2,1)S(1)} collective-permute-done((bf16[256,1024]{1,0:T(8,128)(2,1)S(1)}, bf16[256,1024]{1,0:T(8,128)(2,1)S(1)}, u32[]{:S(2)}, u32[]{:S(2)}) %collective-permute-start.25) | collective-permute-done | bytes 524320 | tf_op jit(solution)/shard_map/ppermute | solution.py:224
  86.1 0.8 copy-done.19
  86.9 1.7 dynamic-slice_convert_fusion
  88.8 25.4 %collective-permute-done.26.refs_8_ = bf16[256,1024]{1,0:T(8,128)(2,1)S(1)} collective-permute-done((bf16[256,1024]{1,0:T(8,128)(2,1)S(1)}, bf16[256,1024]{1,0:T(8,128)(2,1)S(1)}, u32[]{:S(2)}, u32[]{:S(2)}) %collective-permute-start.26) | collective-permute-done | bytes 524320 | tf_op jit(solution)/shard_map/ppermute | solution.py:224
  114.2 2.5 collective-permute-start.50
  116.7 33.6 %collective-permute-start.40 = (bf16[1040,256]{1,0:T(8,128)(2,1)S(1)}, bf16[1040,256]{1,0:T(8,128)(2,1)S(1)}, u32[]{:S(2)}, u32[]{:S(2)}) collective-permute-start(bf16[1040,256]{1,0:T(8,128)(2,1)S(1)} %get-tuple-element.35), channel_id=1, source_target_pairs={{0,4},{2,6},{4,0},{6,2},{8,12},{10,14},{12,8},{14,10},{1,5},{3,7},... | collective-permute-start | bytes 1597448 | tf_op jit(solution)/shard_map/ppermute | solution.py:224
  151.0 8.6 %collective-permute-done.49.refs_0_ = bf16[1040,256]{1,0:T(8,128)(2,1)S(1)} collective-permute-done((bf16[1040,256]{1,0:T(8,128)(2,1)S(1)}, bf16[1040,256]{1,0:T(8,128)(2,1)S(1)}, u32[]{:S(2)}, u32[]{:S(2)}) %collective-permute-start.49) | collective-permute-done | bytes 532512 | tf_op jit(solution)/shard_map/ppermute | solution.py:224
  160.2 1.5 collective-permute-start.30
  161.7 8.7 %collective-permute-done.40.refs_1_ = bf16[1040,256]{1,0:T(8,128)(2,1)S(1)} collective-permute-done((bf16[1040,256]{1,0:T(8,128)(2,1)S(1)}, bf16[1040,256]{1,0:T(8,128)(2,1)S(1)}, u32[]{:S(2)}, u32[]{:S(2)}) %collective-permute-start.40) | collective-permute-done | bytes 532512 | tf_op jit(solution)/shard_map/ppermute | solution.py:224
  171.3 3.1 %collective-permute-done.29.refs_11_ = bf16[256,1024]{1,0:T(8,128)(2,1)S(1)} collective-permute-done((bf16[256,1024]{1,0:T(8,128)(2,1)S(1)}, bf16[256,1024]{1,0:T(8,128)(2,1)S(1)}, u32[]{:S(2)}, u32[]{:S(2)}) %collective-permute-start.29) | collective-permute-done | bytes 524320 | tf_op jit(solution)/shard_map/ppermute | solution.py:224
  174.5 11.2 %collective-permute-done.30.refs_12_ = bf16[256,1024]{1,0:T(8,128)(2,1)S(1)} collective-permute-done((bf16[256,1024]{1,0:T(8,128)(2,1)S(1)}, bf16[256,1024]{1,0:T(8,128)(2,1)S(1)}, u32[]{:S(2)}, u32[]{:S(2)}) %collective-permute-start.30) | collective-permute-done | bytes 524320 | tf_op jit(solution)/shard_map/ppermute | solution.py:224
  186.7 9.0 %collective-permute-done.31.refs_13_ = bf16[256,1024]{1,0:T(8,128)(2,1)S(1)} collective-permute-done((bf16[256,1024]{1,0:T(8,128)(2,1)S(1)}, bf16[256,1024]{1,0:T(8,128)(2,1)S(1)}, u32[]{:S(2)}, u32[]{:S(2)}) %collective-permute-start.31) | collective-permute-done | bytes 524320 | tf_op jit(solution)/shard_map/ppermute | solution.py:224
  196.3 1.6 collective-permute-start.42
  198.8 11.9 %collective-permute-done.55.refs_0_ = bf16[1040,256]{1,0:T(8,128)(2,1)S(1)} collective-permute-done((bf16[1040,256]{1,0:T(8,128)(2,1)S(1)}, bf16[1040,256]{1,0:T(8,128)(2,1)S(1)}, u32[]{:S(2)}, u32[]{:S(2)}) %collective-permute-start.55) | collective-permute-done | bytes 532512 | tf_op jit(solution)/shard_map/ppermute | solution.py:224
  211.1 20.5 %collective-permute-done.56.refs_1_ = bf16[1040,256]{1,0:T(8,128)(2,1)} collective-permute-done((bf16[1040,256]{1,0:T(8,128)(2,1)S(1)}, bf16[1040,256]{1,0:T(8,128)(2,1)}, u32[]{:S(2)}, u32[]{:S(2)}) %collective-permute-start.56) | collective-permute-done | bytes 532512 | tf_op jit(solution)/shard_map/ppermute | solution.py:224
  232.8 1.4 collective-permute-start.24
  235.2 11.9 %collective-permute-done.22.refs_3_ = bf16[128,2048]{1,0:T(8,128)(2,1)S(1)} collective-permute-done((bf16[128,2048]{1,0:T(8,128)(2,1)S(1)}, bf16[128,2048]{1,0:T(8,128)(2,1)S(1)}, u32[]{:S(2)}, u32[]{:S(2)}) %collective-permute-start.22) | collective-permute-done | bytes 524320 | tf_op jit(solution)/shard_map/ppermute | solution.py:195
  247.0 10.7 %collective-permute-done.24.refs_5_ = bf16[128,2048]{1,0:T(8,128)(2,1)S(1)} collective-permute-done((bf16[128,2048]{1,0:T(8,128)(2,1)S(1)}, bf16[128,2048]{1,0:T(8,128)(2,1)S(1)}, u32[]{:S(2)}, u32[]{:S(2)}) %collective-permute-start.24) | collective-permute-done | bytes 524320 | tf_op jit(solution)/shard_map/ppermute | solution.py:195
  257.9 0.8 copy-done.36
  258.7 9.6 %up.1.hidden = bf16[512,2048]{1,0:T(8,128)(2,1)} custom-call(s32[4]{0:T(128)} %pad_add_fusion.pos, f32[1,1024]{1,0:T(1,128)} %bitcast.9, f32[1,1024]{1,0:T(1,128)} %copy-done.58, bf16[128,2048]{1,0:T(8,128)(2,1)} %copy-done.4, bf16[128,2048]{1,0:T(8,128)(2,1)} %copy-done.35, bf16[128,2048]{1,0:T(8,128)(2,1)} %copy-done.31, bf16[128,2048]{1,0:T(8,128)(2,1)} %copy-done.36, ...), custom_call_target="tpu_custom_call" | custom-call | tf_op jit(solution)/shard_map/up/pallas_call | solution.py:396
  268.4 7.1 %shard_map.145 = (f32[256,1024]{1,0:T(8,128)}, bf16[256,1024]{1,0:T(8,128)(2,1)}) custom-call(s32[4]{0:T(128)} %pad_add_fusion.pos, bf16[512,2048]{1,0:T(8,128)(2,1)} %up.1.hidden, bf16[1040,256]{1,0:T(8,128)(2,1)} %copy-done.3, bf16[1040,256]{1,0:T(8,128)(2,1)} %copy-done.13, bf16[1040,256]{1,0:T(8,128)(2,1)} %copy-done.14, ...), custom_call_target="tpu_custom_call" | custom-call | tf_op jit(solution)/shard_map/pallas_call | solution.py:434
  276.1 5.0 %shard_map.147 = (f32[256,512]{1,0:T(8,128)}, bf16[256,512]{1,0:T(8,128)(2,1)}) custom-call(s32[4]{0:T(128)} %pad_add_fusion.pos, bf16[512,2048]{1,0:T(8,128)(2,1)} %up.1.hidden, bf16[1040,256]{1,0:T(8,128)(2,1)} %copy-done.16, bf16[1040,256]{1,0:T(8,128)(2,1)} %collective-permute-done.56.refs_1_, bf16[1040,256]{1,0:T(8,128)(2,1)} %collective-permute-done.57.refs_2_, ...), custom_call_target="tpu_custom_call" | custom-call | tf_op jit(solution)/shard_map/pallas_call | solution.py:434
  281.1 1.5 collective-permute-start.59
  282.6 0.7 constant_dynamic-slice_fusion.1
  283.3 5.1 %shard_map.146 = (f32[256,512]{1,0:T(8,128)}, bf16[256,512]{1,0:T(8,128)(2,1)}) custom-call(s32[4]{0:T(128)} %pad_add_fusion.pos, bf16[512,2048]{1,0:T(8,128)(2,1)} %up.1.hidden, bf16[1040,256]{1,0:T(8,128)(2,1)} %copy-done.11, bf16[1040,256]{1,0:T(8,128)(2,1)} %copy-done.12, bf16[1040,256]{1,0:T(8,128)(2,1)} %collective-permute-done.51.refs_2_, ...), custom_call_target="tpu_custom_call" | custom-call | tf_op jit(solution)/shard_map/pallas_call | solution.py:434
  288.5 0.7 collective-permute-start.53
  289.2 6.5 %collective-permute-done.59 = bf16[256,512]{1,0:T(8,128)(2,1)S(1)} collective-permute-done((bf16[256,512]{1,0:T(8,128)(2,1)}, bf16[256,512]{1,0:T(8,128)(2,1)S(1)}, u32[]{:S(2)}, u32[]{:S(2)}) %collective-permute-start.59) | collective-permute-done | bytes 262176 | tf_op jit(solution)/shard_map/ppermute | solution.py:195
  295.7 0.7 collective-permute-start.60
  296.4 1.0 add_convert_fusion.3
  297.4 1.4 collective-permute-start.48
  298.9 1.0 add_convert_fusion.7
  299.9 0.7 collective-permute-start.54
  300.5 1.6 collective-permute-done.60
  302.3 4.1 %collective-permute-done.48 = bf16[128,1024]{1,0:T(8,128)(2,1)S(1)} collective-permute-done((bf16[128,1024]{1,0:T(8,128)(2,1)S(1)}, bf16[128,1024]{1,0:T(8,128)(2,1)S(1)}, u32[]{:S(2)}, u32[]{:S(2)}) %collective-permute-start.48) | collective-permute-done | bytes 262176 | tf_op jit(solution)/shard_map/ppermute | solution.py:224
  306.4 1.1 add_convert_fusion.2.refs_0_
  308.3 1.1 collective-permute-done.62.refs_4_
  310.0 0.7 copy-done.43
  310.7 2.3 final.1
  (221 shorter events, 15.9 us)
Async XLA Ops:
  3.2 26.8 %collective-permute-start = (bf16[128,2048]{1,0:T(8,128)(2,1)S(1)}, bf16[128,2048]{1,0:T(8,128)(2,1)S(1)}, u32[]{:S(2)}, u32[]{:S(2)}) collective-permute-start(bf16[128,2048]{1,0:T(8,128)(2,1)S(1)} %constant_dynamic-slice_fusion.4), channel_id=1, source_target_pairs={{0,16},{16,0},{1,17},{17,1},{2,18},{18,2},{3,19},{19,3},{4,20},{20... | collective-permute-start | bytes 1572872 | tf_op jit(solution)/shard_map/ppermute | solution.py:195
  7.4 22.0 %collective-permute-start.3 = (bf16[256,512]{1,0:T(8,128)(2,1)S(1)}, bf16[256,512]{1,0:T(8,128)(2,1)S(1)}, u32[]{:S(2)}, u32[]{:S(2)}) collective-permute-start(bf16[256,512]{1,0:T(8,128)(2,1)S(1)} %pad_maximum_fusion.2.refs_3_), channel_id=1, source_target_pairs={{0,8},{2,10},{4,12},{6,14},{8,0},{10,2},{12,4},{14,6},{1,9},{3,11}... | collective-permute-start | bytes 786440 | tf_op jit(solution)/shard_map/ppermute | solution.py:224
  10.2 17.8 %collective-permute-start.13 = (bf16[272,256]{1,0:T(8,128)(2,1)S(1)}, bf16[272,256]{1,0:T(8,128)(2,1)}, u32[]{:S(2)}, u32[]{:S(2)}) collective-permute-start(bf16[272,256]{1,0:T(8,128)(2,1)S(1)} %pad_maximum_fusion.3.refs_4_), channel_id=1, source_target_pairs={{0,8},{2,10},{4,12},{6,14},{8,0},{10,2},{12,4},{14,6},{1,9},{3,11}... | collective-permute-start | bytes 417800 | tf_op jit(solution)/shard_map/ppermute | solution.py:224
  10.6 20.0 %collective-permute-start.2 = (bf16[256,512]{1,0:T(8,128)(2,1)S(1)}, bf16[256,512]{1,0:T(8,128)(2,1)S(1)}, u32[]{:S(2)}, u32[]{:S(2)}) collective-permute-start(bf16[256,512]{1,0:T(8,128)(2,1)S(1)} %pad_maximum_fusion.2.refs_3_), channel_id=1, source_target_pairs={{0,4},{2,6},{4,0},{6,2},{8,12},{10,14},{12,8},{14,10},{1,5},{3,7},... | collective-permute-start | bytes 786440 | tf_op jit(solution)/shard_map/ppermute | solution.py:224
  12.2 17.9 %collective-permute-start.12 = (bf16[272,256]{1,0:T(8,128)(2,1)S(1)}, bf16[272,256]{1,0:T(8,128)(2,1)}, u32[]{:S(2)}, u32[]{:S(2)}) collective-permute-start(bf16[272,256]{1,0:T(8,128)(2,1)S(1)} %pad_maximum_fusion.3.refs_4_), channel_id=1, source_target_pairs={{0,4},{2,6},{4,0},{6,2},{8,12},{10,14},{12,8},{14,10},{1,5},{3,7},... | collective-permute-start | bytes 417800 | tf_op jit(solution)/shard_map/ppermute | solution.py:224
  28.0 9.2 %collective-permute-start.5 = (bf16[256,512]{1,0:T(8,128)(2,1)S(1)}, bf16[256,512]{1,0:T(8,128)(2,1)S(1)}, u32[]{:S(2)}, u32[]{:S(2)}) collective-permute-start(bf16[256,512]{1,0:T(8,128)(2,1)S(1)} %pad_maximum_fusion.2.refs_3_), channel_id=1, source_target_pairs={{0,2},{2,0},{4,6},{6,4},{8,10},{10,8},{12,14},{14,12},{1,3},{3,1},... | collective-permute-start | bytes 786440 | tf_op jit(solution)/shard_map/ppermute | solution.py:224
  29.5 9.2 %collective-permute-start.4 = (bf16[256,512]{1,0:T(8,128)(2,1)S(1)}, bf16[256,512]{1,0:T(8,128)(2,1)}, u32[]{:S(2)}, u32[]{:S(2)}) collective-permute-start(bf16[256,512]{1,0:T(8,128)(2,1)S(1)} %collective-permute-done.3.refs_5_), channel_id=1, source_target_pairs={{0,4},{2,6},{4,0},{6,2},{8,12},{10,14},{12,8},{14,10},{1,5},{3,7},... | collective-permute-start | bytes 786440 | tf_op jit(solution)/shard_map/ppermute | solution.py:224
  30.0 25.6 %collective-permute-start.1 = (bf16[128,2048]{1,0:T(8,128)(2,1)S(1)}, bf16[128,2048]{1,0:T(8,128)(2,1)S(1)}, u32[]{:S(2)}, u32[]{:S(2)}) collective-permute-start(bf16[128,2048]{1,0:T(8,128)(2,1)S(1)} %collective-permute-done.refs_1_), channel_id=1, source_target_pairs={{0,1},{1,0},{2,3},{3,2},{4,5},{5,4},{6,7},{7,6},{8,9},{9,8},{10,11... | collective-permute-start | bytes 1572872 | tf_op jit(solution)/shard_map/ppermute | solution.py:195
  30.0 12.7 %collective-permute-start.7 = (bf16[256,512]{1,0:T(8,128)(2,1)S(1)}, bf16[256,512]{1,0:T(8,128)(2,1)S(1)}, u32[]{:S(2)}, u32[]{:S(2)}) collective-permute-start(bf16[256,512]{1,0:T(8,128)(2,1)S(1)} %collective-permute-done.3.refs_5_), channel_id=1, source_target_pairs={{0,2},{2,0},{4,6},{6,4},{8,10},{10,8},{12,14},{14,12},{1,3},{3,1},... | collective-permute-start | bytes 786440 | tf_op jit(solution)/shard_map/ppermute | solution.py:224
  30.6 8.8 %collective-permute-start.14 = (bf16[272,256]{1,0:T(8,128)(2,1)}, bf16[272,256]{1,0:T(8,128)(2,1)S(1)}, u32[]{:S(2)}, u32[]{:S(2)}) collective-permute-start(bf16[272,256]{1,0:T(8,128)(2,1)} %collective-permute-done.13.refs_6_), channel_id=1, source_target_pairs={{0,4},{2,6},{4,0},{6,2},{8,12},{10,14},{12,8},{14,10},{1,5},{3,7},... | collective-permute-start | bytes 417800 | tf_op jit(solution)/shard_map/ppermute | solution.py:224
  37.1 11.3 %collective-permute-start.6 = (bf16[256,512]{1,0:T(8,128)(2,1)S(1)}, bf16[256,512]{1,0:T(8,128)(2,1)}, u32[]{:S(2)}, u32[]{:S(2)}) collective-permute-start(bf16[256,512]{1,0:T(8,128)(2,1)S(1)} %collective-permute-done.2.refs_4_), channel_id=1, source_target_pairs={{0,2},{2,0},{4,6},{6,4},{8,10},{10,8},{12,14},{14,12},{1,3},{3,1},... | collective-permute-start | bytes 786440 | tf_op jit(solution)/shard_map/ppermute | solution.py:224
  38.7 15.4 %collective-permute-start.8 = (bf16[256,512]{1,0:T(8,128)(2,1)}, bf16[256,512]{1,0:T(8,128)(2,1)}, u32[]{:S(2)}, u32[]{:S(2)}) collective-permute-start(bf16[256,512]{1,0:T(8,128)(2,1)} %collective-permute-done.4.refs_6_), channel_id=1, source_target_pairs={{0,2},{2,0},{4,6},{6,4},{8,10},{10,8},{12,14},{14,12},{1,3},{3,1},... | collective-permute-start | bytes 786440 | tf_op jit(solution)/shard_map/ppermute | solution.py:224
  39.4 25.3 %collective-permute-start.15 = (bf16[272,256]{1,0:T(8,128)(2,1)S(1)}, bf16[272,256]{1,0:T(8,128)(2,1)}, u32[]{:S(2)}, u32[]{:S(2)}) collective-permute-start(bf16[272,256]{1,0:T(8,128)(2,1)S(1)} %pad_maximum_fusion.3.refs_4_), channel_id=1, source_target_pairs={{0,2},{2,0},{4,6},{6,4},{8,10},{10,8},{12,14},{14,12},{1,3},{3,1},... | collective-permute-start | bytes 417800 | tf_op jit(solution)/shard_map/ppermute | solution.py:224
  43.5 21.2 %collective-permute-start.17 = (bf16[272,256]{1,0:T(8,128)(2,1)}, bf16[272,256]{1,0:T(8,128)(2,1)}, u32[]{:S(2)}, u32[]{:S(2)}) collective-permute-start(bf16[272,256]{1,0:T(8,128)(2,1)} %collective-permute-done.13.refs_6_), channel_id=1, source_target_pairs={{0,2},{2,0},{4,6},{6,4},{8,10},{10,8},{12,14},{14,12},{1,3},{3,1},... | collective-permute-start | bytes 417800 | tf_op jit(solution)/shard_map/ppermute | solution.py:224
  48.5 19.6 %collective-permute-start.16 = (bf16[272,256]{1,0:T(8,128)(2,1)}, bf16[272,256]{1,0:T(8,128)(2,1)}, u32[]{:S(2)}, u32[]{:S(2)}) collective-permute-start(bf16[272,256]{1,0:T(8,128)(2,1)} %collective-permute-done.12.refs_5_), channel_id=1, source_target_pairs={{0,2},{2,0},{4,6},{6,4},{8,10},{10,8},{12,14},{14,12},{1,3},{3,1},... | collective-permute-start | bytes 417800 | tf_op jit(solution)/shard_map/ppermute | solution.py:224
  54.1 14.6 %collective-permute-start.18 = (bf16[272,256]{1,0:T(8,128)(2,1)}, bf16[272,256]{1,0:T(8,128)(2,1)}, u32[]{:S(2)}, u32[]{:S(2)}) collective-permute-start(bf16[272,256]{1,0:T(8,128)(2,1)} %copy-done.50), channel_id=1, source_target_pairs={{0,2},{2,0},{4,6},{6,4},{8,10},{10,8},{12,14},{14,12},{1,3},{3,1},... | collective-permute-start | bytes 417800 | tf_op jit(solution)/shard_map/ppermute | solution.py:224
  64.2 4.5 %collective-permute-start.10 = (f32[8,512]{1,0:T(8,128)}, f32[8,512]{1,0:T(8,128)S(1)}, u32[]{:S(2)}, u32[]{:S(2)}) collective-permute-start(f32[8,512]{1,0:T(8,128)} %get-tuple-element.16.refs_0_), channel_id=1, source_target_pairs={{0,16},{1,17},{16,0},{17,1},{2,18},{3,19},{18,2},{19,3},{4,20},{5,... | collective-permute-start | bytes 49160 | tf_op jit(solution)/shard_map/ppermute | solution.py:356
  64.7 4.0 %collective-permute-start.11 = (f32[8,512]{1,0:T(8,128)}, f32[8,512]{1,0:T(8,128)S(1)}, u32[]{:S(2)}, u32[]{:S(2)}) collective-permute-start(f32[8,512]{1,0:T(8,128)} %get-tuple-element.16.refs_0_), channel_id=1, source_target_pairs={{0,17},{1,16},{16,1},{17,0},{2,19},{3,18},{18,3},{19,2},{4,21},{5,... | collective-permute-start | bytes 49160 | tf_op jit(solution)/shard_map/ppermute | solution.py:356
  64.7 4.0 %collective-permute-start.9 = (f32[8,512]{1,0:T(8,128)}, f32[8,512]{1,0:T(8,128)S(1)}, u32[]{:S(2)}, u32[]{:S(2)}) collective-permute-start(f32[8,512]{1,0:T(8,128)} %get-tuple-element.16.refs_0_), channel_id=1, source_target_pairs={{0,1},{1,0},{16,17},{17,16},{2,3},{3,2},{18,19},{19,18},{4,5},{5,4... | collective-permute-start | bytes 49160 | tf_op jit(solution)/shard_map/ppermute | solution.py:356
  68.1 18.0 %collective-permute-start.25 = (bf16[256,1024]{1,0:T(8,128)(2,1)S(1)}, bf16[256,1024]{1,0:T(8,128)(2,1)S(1)}, u32[]{:S(2)}, u32[]{:S(2)}) collective-permute-start(bf16[256,1024]{1,0:T(8,128)(2,1)S(1)} %get-tuple-element.29), channel_id=1, source_target_pairs={{0,4},{2,6},{4,0},{6,2},{8,12},{10,14},{12,8},{14,10},{1,5},{3,7},... | collective-permute-start | bytes 1572872 | tf_op jit(solution)/shard_map/ppermute | solution.py:224
  74.0 76.8 %collective-permute-start.19 = (bf16[256,2048]{1,0:T(8,128)(2,1)}, bf16[256,2048]{1,0:T(8,128)(2,1)S(1)}, u32[]{:S(2)}, u32[]{:S(2)}) collective-permute-start(bf16[256,2048]{1,0:T(8,128)(2,1)} %get-tuple-element.18), channel_id=1, source_target_pairs={{0,1},{1,0},{2,3},{3,2},{4,5},{5,4},{6,7},{7,6},{8,9},{9,8},{10,11... | collective-permute-start | bytes 3145736 | tf_op jit(solution)/shard_map/ppermute | solution.py:195
  74.8 4.4 %collective-permute-start.21 = (f32[1,1024]{1,0:T(1,128)S(1)}, f32[1,1024]{1,0:T(1,128)S(1)}, u32[]{:S(2)}, u32[]{:S(2)}) collective-permute-start(f32[1,1024]{1,0:T(1,128)S(1)} %bitcast.8), channel_id=1, source_target_pairs={{0,1},{1,0},{2,3},{3,2},{4,5},{5,4},{6,7},{7,6},{8,9},{9,8},{10,11... | collective-permute-start | bytes 12296 | tf_op jit(solution)/shard_map/ppermute | solution.py:195
  75.3 38.8 %collective-permute-start.26 = (bf16[256,1024]{1,0:T(8,128)(2,1)S(1)}, bf16[256,1024]{1,0:T(8,128)(2,1)S(1)}, u32[]{:S(2)}, u32[]{:S(2)}) collective-permute-start(bf16[256,1024]{1,0:T(8,128)(2,1)S(1)} %get-tuple-element.30.refs_6_), channel_id=1, source_target_pairs={{0,8},{2,10},{4,12},{6,14},{8,0},{10,2},{12,4},{14,6},{1,9},{3,11}... | collective-permute-start | bytes 1572872 | tf_op jit(solution)/shard_map/ppermute | solution.py:224
  78.9 35.3 %collective-permute-start.27 = (bf16[256,1024]{1,0:T(8,128)(2,1)S(1)}, bf16[256,1024]{1,0:T(8,128)(2,1)S(1)}, u32[]{:S(2)}, u32[]{:S(2)}) collective-permute-start(bf16[256,1024]{1,0:T(8,128)(2,1)S(1)} %get-tuple-element.29), channel_id=1, source_target_pairs={{0,12},{2,14},{4,8},{6,10},{8,4},{10,6},{12,0},{14,2},{1,13},{3,15... | collective-permute-start | bytes 1572872 | tf_op jit(solution)/shard_map/ppermute | solution.py:224
  79.2 37.5 %collective-permute-start.28 = (bf16[256,1024]{1,0:T(8,128)(2,1)S(1)}, bf16[256,1024]{1,0:T(8,128)(2,1)S(1)}, u32[]{:S(2)}, u32[]{:S(2)}) collective-permute-start(bf16[256,1024]{1,0:T(8,128)(2,1)S(1)} %get-tuple-element.30.refs_6_), channel_id=1, source_target_pairs={{0,2},{2,0},{4,6},{6,4},{8,10},{10,8},{12,14},{14,12},{1,3},{3,1},... | collective-permute-start | bytes 1572872 | tf_op jit(solution)/shard_map/ppermute | solution.py:224
  86.1 64.3 %collective-permute-start.32 = (bf16[256,1024]{1,0:T(8,128)(2,1)S(1)}, bf16[256,1024]{1,0:T(8,128)(2,1)}, u32[]{:S(2)}, u32[]{:S(2)}) collective-permute-start(bf16[256,1024]{1,0:T(8,128)(2,1)S(1)} %get-tuple-element.30.refs_6_), channel_id=1, source_target_pairs={{0,1},{1,0},{2,3},{3,2},{4,5},{5,4},{6,7},{7,6},{8,9},{9,8},{10,11... | collective-permute-start | bytes 1572872 | tf_op jit(solution)/shard_map/ppermute | solution.py:195
  114.2 45.5 %collective-permute-start.49 = (bf16[1040,256]{1,0:T(8,128)(2,1)S(1)}, bf16[1040,256]{1,0:T(8,128)(2,1)S(1)}, u32[]{:S(2)}, u32[]{:S(2)}) collective-permute-start(bf16[1040,256]{1,0:T(8,128)(2,1)S(1)} %get-tuple-element.36.refs_0_), channel_id=1, source_target_pairs={{0,8},{2,10},{4,12},{6,14},{8,0},{10,2},{12,4},{14,6},{1,9},{3,11}... | collective-permute-start | bytes 1597448 | tf_op jit(solution)/shard_map/ppermute | solution.py:224
  114.2 46.0 %collective-permute-start.50 = (bf16[1040,256]{1,0:T(8,128)(2,1)S(1)}, bf16[1040,256]{1,0:T(8,128)(2,1)S(1)}, u32[]{:S(2)}, u32[]{:S(2)}) collective-permute-start(bf16[1040,256]{1,0:T(8,128)(2,1)S(1)} %get-tuple-element.35), channel_id=1, source_target_pairs={{0,12},{2,14},{4,8},{6,10},{8,4},{10,6},{12,0},{14,2},{1,13},{3,15... | collective-permute-start | bytes 1597448 | tf_op jit(solution)/shard_map/ppermute | solution.py:224
  116.7 53.6 %collective-permute-start.40 = (bf16[1040,256]{1,0:T(8,128)(2,1)S(1)}, bf16[1040,256]{1,0:T(8,128)(2,1)S(1)}, u32[]{:S(2)}, u32[]{:S(2)}) collective-permute-start(bf16[1040,256]{1,0:T(8,128)(2,1)S(1)} %get-tuple-element.35), channel_id=1, source_target_pairs={{0,4},{2,6},{4,0},{6,2},{8,12},{10,14},{12,8},{14,10},{1,5},{3,7},... | collective-permute-start | bytes 1597448 | tf_op jit(solution)/shard_map/ppermute | solution.py:224
  150.4 20.4 %collective-permute-start.41 = (bf16[1040,256]{1,0:T(8,128)(2,1)S(1)}, bf16[1040,256]{1,0:T(8,128)(2,1)S(1)}, u32[]{:S(2)}, u32[]{:S(2)}) collective-permute-start(bf16[1040,256]{1,0:T(8,128)(2,1)S(1)} %get-tuple-element.36.refs_0_), channel_id=1, source_target_pairs={{0,2},{2,0},{4,6},{6,4},{8,10},{10,8},{12,14},{14,12},{1,3},{3,1},... | collective-permute-start | bytes 1597448 | tf_op jit(solution)/shard_map/ppermute | solution.py:224
  150.9 20.4 %collective-permute-start.43 = (bf16[1040,256]{1,0:T(8,128)(2,1)S(1)}, bf16[1040,256]{1,0:T(8,128)(2,1)S(1)}, u32[]{:S(2)}, u32[]{:S(2)}) collective-permute-start(bf16[1040,256]{1,0:T(8,128)(2,1)S(1)} %get-tuple-element.36.refs_0_), channel_id=1, source_target_pairs={{0,1},{1,0},{2,3},{3,2},{4,5},{5,4},{6,7},{7,6},{8,9},{9,8},{10,11... | collective-permute-start | bytes 1597448 | tf_op jit(solution)/shard_map/ppermute | solution.py:195
  159.7 14.8 %collective-permute-start.29 = (bf16[256,1024]{1,0:T(8,128)(2,1)S(1)}, bf16[256,1024]{1,0:T(8,128)(2,1)S(1)}, u32[]{:S(2)}, u32[]{:S(2)}) collective-permute-start(bf16[256,1024]{1,0:T(8,128)(2,1)S(1)} %copy-done.20), channel_id=1, source_target_pairs={{0,2},{2,0},{4,6},{6,4},{8,10},{10,8},{12,14},{14,12},{1,3},{3,1},... | collective-permute-start | bytes 1572872 | tf_op jit(solution)/shard_map/ppermute | solution.py:224
  160.2 25.5 %collective-permute-start.30 = (bf16[256,1024]{1,0:T(8,128)(2,1)S(1)}, bf16[256,1024]{1,0:T(8,128)(2,1)S(1)}, u32[]{:S(2)}, u32[]{:S(2)}) collective-permute-start(bf16[256,1024]{1,0:T(8,128)(2,1)S(1)} %collective-permute-done.26.refs_8_), channel_id=1, source_target_pairs={{0,2},{2,0},{4,6},{6,4},{8,10},{10,8},{12,14},{14,12},{1,3},{3,1},... | collective-permute-start | bytes 1572872 | tf_op jit(solution)/shard_map/ppermute | solution.py:224
  170.4 15.3 %collective-permute-start.20 = (bf16[128,2048]{1,0:T(8,128)(2,1)S(1)}, bf16[128,2048]{1,0:T(8,128)(2,1)S(1)}, u32[]{:S(2)}, u32[]{:S(2)}) collective-permute-start(bf16[128,2048]{1,0:T(8,128)(2,1)S(1)} %add_convert_fusion.1), channel_id=1, source_target_pairs={{0,16},{16,0},{1,17},{17,1},{2,18},{18,2},{3,19},{19,3},{4,20},{20... | collective-permute-start | bytes 1572872 | tf_op jit(solution)/shard_map/ppermute | solution.py:195
  170.8 24.9 %collective-permute-start.31 = (bf16[256,1024]{1,0:T(8,128)(2,1)S(1)}, bf16[256,1024]{1,0:T(8,128)(2,1)S(1)}, u32[]{:S(2)}, u32[]{:S(2)}) collective-permute-start(bf16[256,1024]{1,0:T(8,128)(2,1)S(1)} %collective-permute-done.27.refs_9_), channel_id=1, source_target_pairs={{0,2},{2,0},{4,6},{6,4},{8,10},{10,8},{12,14},{14,12},{1,3},{3,1},... | collective-permute-start | bytes 1572872 | tf_op jit(solution)/shard_map/ppermute | solution.py:224
  171.3 25.0 %collective-permute-start.33 = (bf16[256,1024]{1,0:T(8,128)(2,1)S(1)}, bf16[256,1024]{1,0:T(8,128)(2,1)S(1)}, u32[]{:S(2)}, u32[]{:S(2)}) collective-permute-start(bf16[256,1024]{1,0:T(8,128)(2,1)S(1)} %copy-done.20), channel_id=1, source_target_pairs={{0,1},{1,0},{2,3},{3,2},{4,5},{5,4},{6,7},{7,6},{8,9},{9,8},{10,11... | collective-permute-start | bytes 1572872 | tf_op jit(solution)/shard_map/ppermute | solution.py:195
  174.5 23.4 %collective-permute-start.34 = (bf16[256,1024]{1,0:T(8,128)(2,1)S(1)}, bf16[256,1024]{1,0:T(8,128)(2,1)S(1)}, u32[]{:S(2)}, u32[]{:S(2)}) collective-permute-start(bf16[256,1024]{1,0:T(8,128)(2,1)S(1)} %collective-permute-done.26.refs_8_), channel_id=1, source_target_pairs={{0,1},{1,0},{2,3},{3,2},{4,5},{5,4},{6,7},{7,6},{8,9},{9,8},{10,11... | collective-permute-start | bytes 1572872 | tf_op jit(solution)/shard_map/ppermute | solution.py:195
  185.7 12.2 %collective-permute-start.35 = (bf16[256,1024]{1,0:T(8,128)(2,1)S(1)}, bf16[256,1024]{1,0:T(8,128)(2,1)S(1)}, u32[]{:S(2)}, u32[]{:S(2)}) collective-permute-start(bf16[256,1024]{1,0:T(8,128)(2,1)S(1)} %collective-permute-done.27.refs_9_), channel_id=1, source_target_pairs={{0,1},{1,0},{2,3},{3,2},{4,5},{5,4},{6,7},{7,6},{8,9},{9,8},{10,11... | collective-permute-start | bytes 1572872 | tf_op jit(solution)/shard_map/ppermute | solution.py:195
  185.7 12.8 %collective-permute-start.36 = (bf16[256,1024]{1,0:T(8,128)(2,1)S(1)}, bf16[256,1024]{1,0:T(8,128)(2,1)S(1)}, u32[]{:S(2)}, u32[]{:S(2)}) collective-permute-start(bf16[256,1024]{1,0:T(8,128)(2,1)S(1)} %collective-permute-done.28.refs_10_), channel_id=1, source_target_pairs={{0,1},{1,0},{2,3},{3,2},{4,5},{5,4},{6,7},{7,6},{8,9},{9,8},{10,11... | collective-permute-start | bytes 1572872 | tf_op jit(solution)/shard_map/ppermute | solution.py:195
  195.8 15.0 %collective-permute-start.55 = (bf16[1040,256]{1,0:T(8,128)(2,1)S(1)}, bf16[1040,256]{1,0:T(8,128)(2,1)S(1)}, u32[]{:S(2)}, u32[]{:S(2)}) collective-permute-start(bf16[1040,256]{1,0:T(8,128)(2,1)S(1)} %collective-permute-done.49.refs_0_), channel_id=1, source_target_pairs={{0,2},{2,0},{4,6},{6,4},{8,10},{10,8},{12,14},{14,12},{1,3},{3,1},... | collective-permute-start | bytes 1597448 | tf_op jit(solution)/shard_map/ppermute | solution.py:224
  196.3 35.4 %collective-permute-start.42 = (bf16[1040,256]{1,0:T(8,128)(2,1)S(1)}, bf16[1040,256]{1,0:T(8,128)(2,1)}, u32[]{:S(2)}, u32[]{:S(2)}) collective-permute-start(bf16[1040,256]{1,0:T(8,128)(2,1)S(1)} %collective-permute-done.40.refs_1_), channel_id=1, source_target_pairs={{0,2},{2,0},{4,6},{6,4},{8,10},{10,8},{12,14},{14,12},{1,3},{3,1},... | collective-permute-start | bytes 1597448 | tf_op jit(solution)/shard_map/ppermute | solution.py:224
  197.9 34.3 %collective-permute-start.44 = (bf16[1040,256]{1,0:T(8,128)(2,1)S(1)}, bf16[1040,256]{1,0:T(8,128)(2,1)S(1)}, u32[]{:S(2)}, u32[]{:S(2)}) collective-permute-start(bf16[1040,256]{1,0:T(8,128)(2,1)S(1)} %collective-permute-done.40.refs_1_), channel_id=1, source_target_pairs={{0,1},{1,0},{2,3},{3,2},{4,5},{5,4},{6,7},{7,6},{8,9},{9,8},{10,11... | collective-permute-start | bytes 1597448 | tf_op jit(solution)/shard_map/ppermute | solution.py:195
  197.9 33.7 %collective-permute-start.56 = (bf16[1040,256]{1,0:T(8,128)(2,1)S(1)}, bf16[1040,256]{1,0:T(8,128)(2,1)}, u32[]{:S(2)}, u32[]{:S(2)}) collective-permute-start(bf16[1040,256]{1,0:T(8,128)(2,1)S(1)} %collective-permute-done.50.refs_1_), channel_id=1, source_target_pairs={{0,2},{2,0},{4,6},{6,4},{8,10},{10,8},{12,14},{14,12},{1,3},{3,1},... | collective-permute-start | bytes 1597448 | tf_op jit(solution)/shard_map/ppermute | solution.py:224
  198.5 33.8 %collective-permute-start.45 = (bf16[1040,256]{1,0:T(8,128)(2,1)S(1)}, bf16[1040,256]{1,0:T(8,128)(2,1)S(1)}, u32[]{:S(2)}, u32[]{:S(2)}) collective-permute-start(bf16[1040,256]{1,0:T(8,128)(2,1)S(1)} %collective-permute-done.41.refs_2_), channel_id=1, source_target_pairs={{0,1},{1,0},{2,3},{3,2},{4,5},{5,4},{6,7},{7,6},{8,9},{9,8},{10,11... | collective-permute-start | bytes 1597448 | tf_op jit(solution)/shard_map/ppermute | solution.py:195
  210.7 22.1 %collective-permute-start.23 = (bf16[128,2048]{1,0:T(8,128)(2,1)S(1)}, bf16[128,2048]{1,0:T(8,128)(2,1)S(1)}, u32[]{:S(2)}, u32[]{:S(2)}) collective-permute-start(bf16[128,2048]{1,0:T(8,128)(2,1)S(1)} %fusion.5.refs_2_), channel_id=1, source_target_pairs={{0,4},{2,6},{4,0},{6,2},{8,12},{10,14},{12,8},{14,10},{1,5},{3,7},... | collective-permute-start | bytes 1572872 | tf_op jit(solution)/shard_map/ppermute | solution.py:224
  231.6 2.6 collective-permute-start.37
  231.6 2.7 collective-permute-start.38
  232.1 2.9 collective-permute-start.39
  232.2 14.8 %collective-permute-start.22 = (bf16[128,2048]{1,0:T(8,128)(2,1)S(1)}, bf16[128,2048]{1,0:T(8,128)(2,1)S(1)}, u32[]{:S(2)}, u32[]{:S(2)}) collective-permute-start(bf16[128,2048]{1,0:T(8,128)(2,1)S(1)} %fusion.5.refs_2_), channel_id=1, source_target_pairs={{0,16},{16,0},{1,17},{17,1},{2,18},{18,2},{3,19},{19,3},{4,20},{20... | collective-permute-start | bytes 1572872 | tf_op jit(solution)/shard_map/ppermute | solution.py:195
  232.8 24.9 %collective-permute-start.24 = (bf16[128,2048]{1,0:T(8,128)(2,1)S(1)}, bf16[128,2048]{1,0:T(8,128)(2,1)S(1)}, u32[]{:S(2)}, u32[]{:S(2)}) collective-permute-start(bf16[128,2048]{1,0:T(8,128)(2,1)S(1)} %collective-permute-done.23.refs_4_), channel_id=1, source_target_pairs={{0,16},{16,0},{1,17},{17,1},{2,18},{18,2},{3,19},{19,3},{4,20},{20... | collective-permute-start | bytes 1572872 | tf_op jit(solution)/shard_map/ppermute | solution.py:195
  234.3 34.1 %collective-permute-start.46 = (bf16[1040,256]{1,0:T(8,128)(2,1)}, bf16[1040,256]{1,0:T(8,128)(2,1)}, u32[]{:S(2)}, u32[]{:S(2)}) collective-permute-start(bf16[1040,256]{1,0:T(8,128)(2,1)} %collective-permute-done.42.refs_3_), channel_id=1, source_target_pairs={{0,1},{1,0},{2,3},{3,2},{4,5},{5,4},{6,7},{7,6},{8,9},{9,8},{10,11... | collective-permute-start | bytes 1597448 | tf_op jit(solution)/shard_map/ppermute | solution.py:195
  234.3 41.8 %collective-permute-start.57 = (bf16[1040,256]{1,0:T(8,128)(2,1)S(1)}, bf16[1040,256]{1,0:T(8,128)(2,1)}, u32[]{:S(2)}, u32[]{:S(2)}) collective-permute-start(bf16[1040,256]{1,0:T(8,128)(2,1)S(1)} %collective-permute-done.55.refs_0_), channel_id=1, source_target_pairs={{0,1},{1,0},{2,3},{3,2},{4,5},{5,4},{6,7},{7,6},{8,9},{9,8},{10,11... | collective-permute-start | bytes 1597448 | tf_op jit(solution)/shard_map/ppermute | solution.py:195
  235.0 41.1 %collective-permute-start.58 = (bf16[1040,256]{1,0:T(8,128)(2,1)}, bf16[1040,256]{1,0:T(8,128)(2,1)}, u32[]{:S(2)}, u32[]{:S(2)}) collective-permute-start(bf16[1040,256]{1,0:T(8,128)(2,1)} %collective-permute-done.56.refs_1_), channel_id=1, source_target_pairs={{0,1},{1,0},{2,3},{3,2},{4,5},{5,4},{6,7},{7,6},{8,9},{9,8},{10,11... | collective-permute-start | bytes 1597448 | tf_op jit(solution)/shard_map/ppermute | solution.py:195
  247.0 36.2 %collective-permute-start.51 = (bf16[1040,256]{1,0:T(8,128)(2,1)S(1)}, bf16[1040,256]{1,0:T(8,128)(2,1)}, u32[]{:S(2)}, u32[]{:S(2)}) collective-permute-start(bf16[1040,256]{1,0:T(8,128)(2,1)S(1)} %collective-permute-done.49.refs_0_), channel_id=1, source_target_pairs={{0,1},{1,0},{2,3},{3,2},{4,5},{5,4},{6,7},{7,6},{8,9},{9,8},{10,11... | collective-permute-start | bytes 1597448 | tf_op jit(solution)/shard_map/ppermute | solution.py:195
  258.7 24.6 %collective-permute-start.52 = (bf16[1040,256]{1,0:T(8,128)(2,1)S(1)}, bf16[1040,256]{1,0:T(8,128)(2,1)}, u32[]{:S(2)}, u32[]{:S(2)}) collective-permute-start(bf16[1040,256]{1,0:T(8,128)(2,1)S(1)} %collective-permute-done.50.refs_1_), channel_id=1, source_target_pairs={{0,1},{1,0},{2,3},{3,2},{4,5},{5,4},{6,7},{7,6},{8,9},{9,8},{10,11... | collective-permute-start | bytes 1597448 | tf_op jit(solution)/shard_map/ppermute | solution.py:195
  275.5 21.0 %collective-permute-start.47 = (bf16[256,1024]{1,0:T(8,128)(2,1)}, bf16[256,1024]{1,0:T(8,128)(2,1)}, u32[]{:S(2)}, u32[]{:S(2)}) collective-permute-start(bf16[256,1024]{1,0:T(8,128)(2,1)} %get-tuple-element.20), channel_id=1, source_target_pairs={{0,16},{16,0},{1,17},{17,1},{2,18},{18,2},{3,19},{19,3},{4,20},{20... | collective-permute-start | bytes 1572872 | tf_op jit(solution)/shard_map/ppermute | solution.py:195
  281.1 14.6 %collective-permute-start.59 = (bf16[256,512]{1,0:T(8,128)(2,1)}, bf16[256,512]{1,0:T(8,128)(2,1)S(1)}, u32[]{:S(2)}, u32[]{:S(2)}) collective-permute-start(bf16[256,512]{1,0:T(8,128)(2,1)} %get-tuple-element.24), channel_id=1, source_target_pairs={{0,16},{16,0},{1,17},{17,1},{2,18},{18,2},{3,19},{19,3},{4,20},{20... | collective-permute-start | bytes 786440 | tf_op jit(solution)/shard_map/ppermute | solution.py:195
  288.5 10.4 %collective-permute-start.53 = (bf16[256,512]{1,0:T(8,128)(2,1)}, bf16[256,512]{1,0:T(8,128)(2,1)S(1)}, u32[]{:S(2)}, u32[]{:S(2)}) collective-permute-start(bf16[256,512]{1,0:T(8,128)(2,1)} %get-tuple-element.22), channel_id=1, source_target_pairs={{0,4},{2,6},{4,0},{6,2},{8,12},{10,14},{12,8},{14,10},{1,5},{3,7},... | collective-permute-start | bytes 786440 | tf_op jit(solution)/shard_map/ppermute | solution.py:224
  295.7 6.4 %collective-permute-start.60 = (bf16[128,512]{1,0:T(8,128)(2,1)S(1)}, bf16[128,512]{1,0:T(8,128)(2,1)S(1)}, u32[]{:S(2)}, u32[]{:S(2)}) collective-permute-start(bf16[128,512]{1,0:T(8,128)(2,1)S(1)} %add_convert_fusion.5), channel_id=1, source_target_pairs={{0,4},{2,6},{4,0},{6,2},{8,12},{10,14},{12,8},{14,10},{1,5},{3,7},... | collective-permute-start | bytes 393224 | tf_op jit(solution)/shard_map/ppermute | solution.py:224
  297.4 9.0 %collective-permute-start.48 = (bf16[128,1024]{1,0:T(8,128)(2,1)S(1)}, bf16[128,1024]{1,0:T(8,128)(2,1)S(1)}, u32[]{:S(2)}, u32[]{:S(2)}) collective-permute-start(bf16[128,1024]{1,0:T(8,128)(2,1)S(1)} %add_convert_fusion.3), channel_id=1, source_target_pairs={{0,4},{2,6},{4,0},{6,2},{8,12},{10,14},{12,8},{14,10},{1,5},{3,7},... | collective-permute-start | bytes 786440 | tf_op jit(solution)/shard_map/ppermute | solution.py:224
  299.9 7.7 %collective-permute-start.54 = (bf16[128,512]{1,0:T(8,128)(2,1)S(1)}, bf16[128,512]{1,0:T(8,128)(2,1)S(1)}, u32[]{:S(2)}, u32[]{:S(2)}) collective-permute-start(bf16[128,512]{1,0:T(8,128)(2,1)S(1)} %add_convert_fusion.7), channel_id=1, source_target_pairs={{0,16},{16,0},{1,17},{17,1},{2,18},{18,2},{3,19},{19,3},{4,20},{20... | collective-permute-start | bytes 393224 | tf_op jit(solution)/shard_map/ppermute | solution.py:195
  302.2 6.0 %collective-permute-start.63 = (bf16[128,512]{1,0:T(8,128)(2,1)S(1)}, bf16[128,512]{1,0:T(8,128)(2,1)S(1)}, u32[]{:S(2)}, u32[]{:S(2)}) collective-permute-start(bf16[128,512]{1,0:T(8,128)(2,1)S(1)} %add_convert_fusion.4.refs_2_), channel_id=1, source_target_pairs={{0,1},{1,0},{2,3},{3,2},{4,5},{5,4},{6,7},{7,6},{8,9},{9,8},{10,11... | collective-permute-start | bytes 393224 | tf_op jit(solution)/shard_map/ppermute | solution.py:195
  307.5 1.8 collective-permute-start.61
  307.7 1.6 collective-permute-start.62
  (61 other events, 2611.8 us)
where the time goes:
time: 314 us; the launch traced here: 313 us
  waiting for transfers between devices  171 us (54%)
  starting transfers between devices  80.9 us (26%)
  Pallas kernels  41.5 us (13%)
  local copies, waits for them, and re-layouts  11.3 us (4%)
  other arithmetic  7.85 us (2%)
    ppermute x32, waiting for transfers between devices, along(): lax.ppermute(a, 'fs', [(o * inner + i, to(o, i)) for o in range(outer) fo...  140 us
    ppermute x32, starting transfers between devices, along(): lax.ppermute(a, 'fs', [(o * inner + i, to(o, i)) for o in range(outer) fo...  67.2 us
    ppermute x29, waiting for transfers between devices, shift(): lax.ppermute(array, axis, [(i, (i + by) % size) for i in range(size)])  30.4 us
    pallas_call x3, Pallas kernels, on_device(): pl.pallas_call(functools.partial(down_kernel, at, tps, order, n, size), o...  17.2 us
    ppermute x29, starting transfers between devices, shift(): lax.ppermute(array, axis, [(i, (i + by) % size) for i in range(size)])  11.5 us
    pallas_call x1, Pallas kernels, on_device(): pl.pallas_call(functools.partial(up_kernel, all_places, len(toks), tps),...  9.61 us
    pallas_call x1, Pallas kernels, on_device(): pl.pallas_call(functools.partial(glu_conv_kernel, all_places, offsets, ro...  7.73 us
  transfers between devices with their start and end apart: 64, of which 22 were waited for; matrix products, arithmetic and copies ran while one was open for 3% of the time, Pallas kernels for 13%

commit v1 on v0

--- a/solution.py
+++ b/solution.py
@@ -174,20 +174,22 @@
 
 
 def final_kernel(inner, pair, cols, tps, pos, *refs):
-    out = refs[-1]
+    out, sems = refs[-2:]
     n_parts = 1 + inner
+    pairs = []
     base = pos[1] - lax.rem(pos[1], pair)
     for c in range(tps):
         parts = refs[c * n_parts : (c + 1) * n_parts]
         n = parts[0].shape[0]
         rows = pl.ds(pl.multiple_of(lax.rem(pos[3] + tps - c, tps) * n, n), n)
         wide = parts[0].shape[1]
-        out[rows, pl.ds(pl.multiple_of(base * inner * cols, cols), wide)] = parts[0][...]
+        pairs.append((parts[0], out.at[rows, pl.ds(pl.multiple_of(base * inner * cols, cols), wide)]))
         for k in range(inner):
             for z in range(pair):
                 block = (pair - base + z) * inner + lax.rem(pos[2] + inner - k, inner)
                 at = pl.multiple_of(block * cols, cols)
-                out[rows, pl.ds(at, cols)] = parts[1 + k][:, z * cols : (z + 1) * cols]
+                pairs.append((parts[1 + k].at[:, pl.ds(z * cols, cols)], out.at[rows, pl.ds(at, cols)]))
+    wait_all(start_all(pairs, sems))
 
 
 def shift(array, axis, by):
@@ -476,8 +478,9 @@
         return pl.pallas_call(
             functools.partial(final_kernel, inner, pair, block_cols, tps),
             out_shape=jax.ShapeDtypeStruct((count, width), BF16),
-            in_specs=[SMEM] + [VMEM] * (len(results) * tps),
-            out_specs=VMEM,
+            in_specs=[SMEM] + [ANY] * (len(results) * tps),
+            out_specs=ANY,
+            scratch_shapes=[pltpu.SemaphoreType.DMA((tps * (1 + inner * pair),))],
             name="final",
         )(pos, *[a for row in pieces for a in row])
     result = jnp.zeros((count, width), BF16)

time: 314 us -> 345 us (1.099)
  Pallas kernels: 41.5 us -> 72.9 us
    pallas_call x1, Pallas kernels: 2.28 us -> 33.6 us  [on_device(): pl.pallas_call(functools.partial(final_kernel, inner, pair, block_cols, t...]
  transfers between devices with their start and end apart: 64 -> 64, of which waited for: 22 -> 22; matrix products, arithmetic and copies ran while one was open for 3% -> 3% of each run, Pallas kernels for 13% -> 11%
where the time goes in v1:
time: 345 us; the launch traced here: 344 us
  waiting for transfers between devices  171 us (50%)
  starting transfers between devices  80.9 us (23%)
  Pallas kernels  72.9 us (21%)
  local copies, waits for them, and re-layouts  11.3 us (3%)
  other arithmetic  7.85 us (2%)
    ppermute x32, waiting for transfers between devices, along(): lax.ppermute(a, 'fs', [(o * inner + i, to(o, i)) for o in range(outer) fo...  140 us
    ppermute x32, starting transfers between devices, along(): lax.ppermute(a, 'fs', [(o * inner + i, to(o, i)) for o in range(outer) fo...  67.2 us
    pallas_call x1, Pallas kernels, on_device(): pl.pallas_call(functools.partial(final_kernel, inner, pair, block_cols, t...  33.6 us
    ppermute x29, waiting for transfers between devices, shift(): lax.ppermute(array, axis, [(i, (i + by) % size) for i in range(size)])  30.4 us
    pallas_call x3, Pallas kernels, on_device(): pl.pallas_call(functools.partial(down_kernel, at, tps, order, n, size), o...  17.2 us
    ppermute x29, starting transfers between devices, shift(): lax.ppermute(array, axis, [(i, (i + by) % size) for i in range(size)])  11.5 us
    pallas_call x1, Pallas kernels, on_device(): pl.pallas_call(functools.partial(up_kernel, all_places, len(toks), tps),...  9.61 us
    pallas_call x1, Pallas kernels, on_device(): pl.pallas_call(functools.partial(glu_conv_kernel, all_places, offsets, ro...  7.73 us
  transfers between devices with their start and end apart: 64, of which 22 were waited for; matrix products, arithmetic and copies ran while one was open for 3% of the time, Pallas kernels for 11%

profile of v1, /device:TPU:0, one launch (start us, length us, event | category | flops | bytes accessed | tf_op | source)
XLA Modules:
  0.0 344.5 jit_solution(2760724410087252770)
XLA Ops:
  0.0 1.6 fusion
  1.6 1.5 fusion.2.refs_0_
  3.2 3.0 collective-permute-start
  6.2 1.2 dynamic-slice_convert_fusion.5
  7.4 2.7 collective-permute-start.3
  10.6 1.6 collective-permute-start.2
  12.6 15.4 %collective-permute-done.13.refs_6_ = bf16[272,256]{1,0:T(8,128)(2,1)} collective-permute-done((bf16[272,256]{1,0:T(8,128)(2,1)S(1)}, bf16[272,256]{1,0:T(8,128)(2,1)}, u32[]{:S(2)}, u32[]{:S(2)}) %collective-permute-start.13) | collective-permute-done | bytes 139296 | tf_op jit(solution)/shard_map/ppermute | solution.py:226
  28.0 1.5 collective-permute-start.5
  30.6 1.5 collective-permute-start.14
  32.1 5.0 %collective-permute-done.5.refs_7_ = bf16[256,512]{1,0:T(8,128)(2,1)S(1)} collective-permute-done((bf16[256,512]{1,0:T(8,128)(2,1)S(1)}, bf16[256,512]{1,0:T(8,128)(2,1)S(1)}, u32[]{:S(2)}, u32[]{:S(2)}) %collective-permute-start.5) | collective-permute-done | bytes 262176 | tf_op jit(solution)/shard_map/ppermute | solution.py:226
  37.1 1.5 collective-permute-start.6
  39.4 1.3 collective-permute-start.15
  40.7 2.0 collective-permute-done.7.refs_9_
  42.8 0.7 copy-done.49
  43.5 1.5 collective-permute-start.17
  45.6 2.8 collective-permute-done.6.refs_8_
  48.5 1.5 collective-permute-start.16
  50.0 4.1 %collective-permute-done.8.refs_10_ = bf16[256,512]{1,0:T(8,128)(2,1)} collective-permute-done((bf16[256,512]{1,0:T(8,128)(2,1)}, bf16[256,512]{1,0:T(8,128)(2,1)}, u32[]{:S(2)}, u32[]{:S(2)}) %collective-permute-start.8) | collective-permute-done | bytes 262176 | tf_op jit(solution)/shard_map/ppermute | solution.py:226
  54.1 1.5 collective-permute-start.18
  55.7 0.8 copy-done.42
  56.4 7.7 %glu_conv.1 = (f32[512,256]{1,0:T(8,128)}, f32[8,512]{1,0:T(8,128)}) custom-call(s32[4]{0:T(128)} %pad_add_fusion.pos, f32[1,512]{1,0:T(1,128)} %bitcast.10, f32[1,512]{1,0:T(1,128)} %bitcast.11, f32[31,512]{1,0:T(8,128)} %taps.1, bf16[256,2048]{1,0:T(8,128)(2,1)} %copy-done.2, bf16[128,2048]{1,0:T(8,128)(2,1)} %copy-done.41, bf16[128,2048]{1,0:T(8,128)(2,1)} %copy-done.42, ...), custom_call_target="tpu_custom_call" | custom-call | tf_op jit(solution)/shard_map/glu_conv/pallas_call | solution.py:332
  64.7 1.7 collective-permute-start.9
  66.4 1.7 dynamic-slice_convert_fusion.2
  69.3 4.7 %mix.1 = (bf16[256,2048]{1,0:T(8,128)(2,1)}, bf16[256,2048]{1,0:T(8,128)(2,1)}) custom-call(s32[4]{0:T(128)} %pad_add_fusion.pos, f32[1,512]{1,0:T(1,128)} %bitcast.12, f32[512,256]{1,0:T(8,128)} %get-tuple-element.15.conv, f32[8,512]{1,0:T(8,128)} %get-tuple-element.16.refs_0_, f32[8,512]{1,0:T(8,128)} %copy-done.55, f32[8,512]{1,0:T(8,128)} %copy-done.53, ...), custom_call_target="tpu_custom_call" | custom-call | tf_op jit(solution)/shard_map/mix/pallas_call | solution.py:362
  74.1 0.7 dynamic_slice.51
  75.3 3.5 %collective-permute-start.26 = (bf16[256,1024]{1,0:T(8,128)(2,1)S(1)}, bf16[256,1024]{1,0:T(8,128)(2,1)S(1)}, u32[]{:S(2)}, u32[]{:S(2)}) collective-permute-start(bf16[256,1024]{1,0:T(8,128)(2,1)S(1)} %get-tuple-element.30.refs_6_), channel_id=1, source_target_pairs={{0,8},{2,10},{4,12},{6,14},{8,0},{10,2},{12,4},{14,6},{1,9},{3,11}... | collective-permute-start | bytes 1572872 | tf_op jit(solution)/shard_map/ppermute | solution.py:226
  79.7 6.4 %collective-permute-done.25.refs_7_ = bf16[256,1024]{1,0:T(8,128)(2,1)S(1)} collective-permute-done((bf16[256,1024]{1,0:T(8,128)(2,1)S(1)}, bf16[256,1024]{1,0:T(8,128)(2,1)S(1)}, u32[]{:S(2)}, u32[]{:S(2)}) %collective-permute-start.25) | collective-permute-done | bytes 524320 | tf_op jit(solution)/shard_map/ppermute | solution.py:226
  86.1 0.8 copy-done.19
  86.9 1.7 dynamic-slice_convert_fusion
  88.8 25.4 %collective-permute-done.26.refs_8_ = bf16[256,1024]{1,0:T(8,128)(2,1)S(1)} collective-permute-done((bf16[256,1024]{1,0:T(8,128)(2,1)S(1)}, bf16[256,1024]{1,0:T(8,128)(2,1)S(1)}, u32[]{:S(2)}, u32[]{:S(2)}) %collective-permute-start.26) | collective-permute-done | bytes 524320 | tf_op jit(solution)/shard_map/ppermute | solution.py:226
  114.2 2.5 collective-permute-start.50
  116.7 33.6 %collective-permute-start.40 = (bf16[1040,256]{1,0:T(8,128)(2,1)S(1)}, bf16[1040,256]{1,0:T(8,128)(2,1)S(1)}, u32[]{:S(2)}, u32[]{:S(2)}) collective-permute-start(bf16[1040,256]{1,0:T(8,128)(2,1)S(1)} %get-tuple-element.35), channel_id=1, source_target_pairs={{0,4},{2,6},{4,0},{6,2},{8,12},{10,14},{12,8},{14,10},{1,5},{3,7},... | collective-permute-start | bytes 1597448 | tf_op jit(solution)/shard_map/ppermute | solution.py:226
  151.0 8.6 %collective-permute-done.49.refs_0_ = bf16[1040,256]{1,0:T(8,128)(2,1)S(1)} collective-permute-done((bf16[1040,256]{1,0:T(8,128)(2,1)S(1)}, bf16[1040,256]{1,0:T(8,128)(2,1)S(1)}, u32[]{:S(2)}, u32[]{:S(2)}) %collective-permute-start.49) | collective-permute-done | bytes 532512 | tf_op jit(solution)/shard_map/ppermute | solution.py:226
  160.2 1.5 collective-permute-start.30
  161.7 8.7 %collective-permute-done.40.refs_1_ = bf16[1040,256]{1,0:T(8,128)(2,1)S(1)} collective-permute-done((bf16[1040,256]{1,0:T(8,128)(2,1)S(1)}, bf16[1040,256]{1,0:T(8,128)(2,1)S(1)}, u32[]{:S(2)}, u32[]{:S(2)}) %collective-permute-start.40) | collective-permute-done | bytes 532512 | tf_op jit(solution)/shard_map/ppermute | solution.py:226
  171.3 3.1 collective-permute-done.29.refs_11_
  174.5 11.2 %collective-permute-done.30.refs_12_ = bf16[256,1024]{1,0:T(8,128)(2,1)S(1)} collective-permute-done((bf16[256,1024]{1,0:T(8,128)(2,1)S(1)}, bf16[256,1024]{1,0:T(8,128)(2,1)S(1)}, u32[]{:S(2)}, u32[]{:S(2)}) %collective-permute-start.30) | collective-permute-done | bytes 524320 | tf_op jit(solution)/shard_map/ppermute | solution.py:226
  186.7 9.0 %collective-permute-done.31.refs_13_ = bf16[256,1024]{1,0:T(8,128)(2,1)S(1)} collective-permute-done((bf16[256,1024]{1,0:T(8,128)(2,1)S(1)}, bf16[256,1024]{1,0:T(8,128)(2,1)S(1)}, u32[]{:S(2)}, u32[]{:S(2)}) %collective-permute-start.31) | collective-permute-done | bytes 524320 | tf_op jit(solution)/shard_map/ppermute | solution.py:226
  196.3 1.6 collective-permute-start.42
  198.8 11.9 %collective-permute-done.55.refs_0_ = bf16[1040,256]{1,0:T(8,128)(2,1)S(1)} collective-permute-done((bf16[1040,256]{1,0:T(8,128)(2,1)S(1)}, bf16[1040,256]{1,0:T(8,128)(2,1)S(1)}, u32[]{:S(2)}, u32[]{:S(2)}) %collective-permute-start.55) | collective-permute-done | bytes 532512 | tf_op jit(solution)/shard_map/ppermute | solution.py:226
  211.1 20.5 %collective-permute-done.56.refs_1_ = bf16[1040,256]{1,0:T(8,128)(2,1)} collective-permute-done((bf16[1040,256]{1,0:T(8,128)(2,1)S(1)}, bf16[1040,256]{1,0:T(8,128)(2,1)}, u32[]{:S(2)}, u32[]{:S(2)}) %collective-permute-start.56) | collective-permute-done | bytes 532512 | tf_op jit(solution)/shard_map/ppermute | solution.py:226
  232.8 1.4 collective-permute-start.24
  235.2 11.9 %collective-permute-done.22.refs_3_ = bf16[128,2048]{1,0:T(8,128)(2,1)S(1)} collective-permute-done((bf16[128,2048]{1,0:T(8,128)(2,1)S(1)}, bf16[128,2048]{1,0:T(8,128)(2,1)S(1)}, u32[]{:S(2)}, u32[]{:S(2)}) %collective-permute-start.22) | collective-permute-done | bytes 524320 | tf_op jit(solution)/shard_map/ppermute | solution.py:197
  247.0 10.7 %collective-permute-done.24.refs_5_ = bf16[128,2048]{1,0:T(8,128)(2,1)S(1)} collective-permute-done((bf16[128,2048]{1,0:T(8,128)(2,1)S(1)}, bf16[128,2048]{1,0:T(8,128)(2,1)S(1)}, u32[]{:S(2)}, u32[]{:S(2)}) %collective-permute-start.24) | collective-permute-done | bytes 524320 | tf_op jit(solution)/shard_map/ppermute | solution.py:197
  257.9 0.8 copy-done.36
  258.7 9.6 %up.1.hidden = bf16[512,2048]{1,0:T(8,128)(2,1)} custom-call(s32[4]{0:T(128)} %pad_add_fusion.pos, f32[1,1024]{1,0:T(1,128)} %bitcast.9, f32[1,1024]{1,0:T(1,128)} %copy-done.58, bf16[128,2048]{1,0:T(8,128)(2,1)} %copy-done.4, bf16[128,2048]{1,0:T(8,128)(2,1)} %copy-done.35, bf16[128,2048]{1,0:T(8,128)(2,1)} %copy-done.31, bf16[128,2048]{1,0:T(8,128)(2,1)} %copy-done.36, ...), custom_call_target="tpu_custom_call" | custom-call | tf_op jit(solution)/shard_map/up/pallas_call | solution.py:398
  268.4 7.1 %shard_map.145 = (f32[256,1024]{1,0:T(8,128)}, bf16[256,1024]{1,0:T(8,128)(2,1)}) custom-call(s32[4]{0:T(128)} %pad_add_fusion.pos, bf16[512,2048]{1,0:T(8,128)(2,1)} %up.1.hidden, bf16[1040,256]{1,0:T(8,128)(2,1)} %copy-done.3, bf16[1040,256]{1,0:T(8,128)(2,1)} %copy-done.13, bf16[1040,256]{1,0:T(8,128)(2,1)} %copy-done.14, ...), custom_call_target="tpu_custom_call" | custom-call | tf_op jit(solution)/shard_map/pallas_call | solution.py:436
  276.1 5.0 %shard_map.147 = (f32[256,512]{1,0:T(8,128)}, bf16[256,512]{1,0:T(8,128)(2,1)}) custom-call(s32[4]{0:T(128)} %pad_add_fusion.pos, bf16[512,2048]{1,0:T(8,128)(2,1)} %up.1.hidden, bf16[1040,256]{1,0:T(8,128)(2,1)} %copy-done.16, bf16[1040,256]{1,0:T(8,128)(2,1)} %collective-permute-done.56.refs_1_, bf16[1040,256]{1,0:T(8,128)(2,1)} %collective-permute-done.57.refs_2_, ...), custom_call_target="tpu_custom_call" | custom-call | tf_op jit(solution)/shard_map/pallas_call | solution.py:436
  281.1 1.5 collective-permute-start.59
  282.6 0.7 constant_dynamic-slice_fusion.1
  283.3 5.1 %shard_map.146 = (f32[256,512]{1,0:T(8,128)}, bf16[256,512]{1,0:T(8,128)(2,1)}) custom-call(s32[4]{0:T(128)} %pad_add_fusion.pos, bf16[512,2048]{1,0:T(8,128)(2,1)} %up.1.hidden, bf16[1040,256]{1,0:T(8,128)(2,1)} %copy-done.11, bf16[1040,256]{1,0:T(8,128)(2,1)} %copy-done.12, bf16[1040,256]{1,0:T(8,128)(2,1)} %collective-permute-done.51.refs_2_, ...), custom_call_target="tpu_custom_call" | custom-call | tf_op jit(solution)/shard_map/pallas_call | solution.py:436
  288.5 0.7 collective-permute-start.53
  289.2 6.5 %collective-permute-done.59 = bf16[256,512]{1,0:T(8,128)(2,1)S(1)} collective-permute-done((bf16[256,512]{1,0:T(8,128)(2,1)}, bf16[256,512]{1,0:T(8,128)(2,1)S(1)}, u32[]{:S(2)}, u32[]{:S(2)}) %collective-permute-start.59) | collective-permute-done | bytes 262176 | tf_op jit(solution)/shard_map/ppermute | solution.py:197
  295.7 0.7 collective-permute-start.60
  296.4 1.0 add_convert_fusion.3
  297.4 1.4 collective-permute-start.48
  298.9 1.0 add_convert_fusion.7
  299.9 0.7 collective-permute-start.54
  300.5 1.6 collective-permute-done.60
  302.3 4.1 %collective-permute-done.48 = bf16[128,1024]{1,0:T(8,128)(2,1)S(1)} collective-permute-done((bf16[128,1024]{1,0:T(8,128)(2,1)S(1)}, bf16[128,1024]{1,0:T(8,128)(2,1)S(1)}, u32[]{:S(2)}, u32[]{:S(2)}) %collective-permute-start.48) | collective-permute-done | bytes 262176 | tf_op jit(solution)/shard_map/ppermute | solution.py:226
  306.4 1.1 add_convert_fusion.2.refs_0_
  308.3 1.1 collective-permute-done.62.refs_4_
  310.0 0.7 copy-done.43
  310.7 33.6 %final.1 = bf16[256,2048]{1,0:T(8,128)(2,1)} custom-call(s32[4]{0:T(128)} %pad_add_fusion.pos, bf16[128,1024]{1,0:T(8,128)(2,1)} %copy-done.8, bf16[128,512]{1,0:T(8,128)(2,1)} %copy-done.40, bf16[128,512]{1,0:T(8,128)(2,1)} %copy-done.39, bf16[128,1024]{1,0:T(8,128)(2,1)} %copy-done.43, bf16[128,512]{1,0:T(8,128)(2,1)} %copy-done.52, ...), custom_call_target="tpu_custom_call" | custom-call | tf_op jit(solution)/shard_map/final/pallas_call | solution.py:478
  (221 shorter events, 15.9 us)
Async XLA Ops:
  3.2 26.8 %collective-permute-start = (bf16[128,2048]{1,0:T(8,128)(2,1)S(1)}, bf16[128,2048]{1,0:T(8,128)(2,1)S(1)}, u32[]{:S(2)}, u32[]{:S(2)}) collective-permute-start(bf16[128,2048]{1,0:T(8,128)(2,1)S(1)} %constant_dynamic-slice_fusion.4), channel_id=1, source_target_pairs={{0,16},{16,0},{1,17},{17,1},{2,18},{18,2},{3,19},{19,3},{4,20},{20... | collective-permute-start | bytes 1572872 | tf_op jit(solution)/shard_map/ppermute | solution.py:197
  7.4 22.0 %collective-permute-start.3 = (bf16[256,512]{1,0:T(8,128)(2,1)S(1)}, bf16[256,512]{1,0:T(8,128)(2,1)S(1)}, u32[]{:S(2)}, u32[]{:S(2)}) collective-permute-start(bf16[256,512]{1,0:T(8,128)(2,1)S(1)} %pad_maximum_fusion.2.refs_3_), channel_id=1, source_target_pairs={{0,8},{2,10},{4,12},{6,14},{8,0},{10,2},{12,4},{14,6},{1,9},{3,11}... | collective-permute-start | bytes 786440 | tf_op jit(solution)/shard_map/ppermute | solution.py:226
  10.2 17.8 %collective-permute-start.13 = (bf16[272,256]{1,0:T(8,128)(2,1)S(1)}, bf16[272,256]{1,0:T(8,128)(2,1)}, u32[]{:S(2)}, u32[]{:S(2)}) collective-permute-start(bf16[272,256]{1,0:T(8,128)(2,1)S(1)} %pad_maximum_fusion.3.refs_4_), channel_id=1, source_target_pairs={{0,8},{2,10},{4,12},{6,14},{8,0},{10,2},{12,4},{14,6},{1,9},{3,11}... | collective-permute-start | bytes 417800 | tf_op jit(solution)/shard_map/ppermute | solution.py:226
  10.6 20.0 %collective-permute-start.2 = (bf16[256,512]{1,0:T(8,128)(2,1)S(1)}, bf16[256,512]{1,0:T(8,128)(2,1)S(1)}, u32[]{:S(2)}, u32[]{:S(2)}) collective-permute-start(bf16[256,512]{1,0:T(8,128)(2,1)S(1)} %pad_maximum_fusion.2.refs_3_), channel_id=1, source_target_pairs={{0,4},{2,6},{4,0},{6,2},{8,12},{10,14},{12,8},{14,10},{1,5},{3,7},... | collective-permute-start | bytes 786440 | tf_op jit(solution)/shard_map/ppermute | solution.py:226
  12.2 17.9 %collective-permute-start.12 = (bf16[272,256]{1,0:T(8,128)(2,1)S(1)}, bf16[272,256]{1,0:T(8,128)(2,1)}, u32[]{:S(2)}, u32[]{:S(2)}) collective-permute-start(bf16[272,256]{1,0:T(8,128)(2,1)S(1)} %pad_maximum_fusion.3.refs_4_), channel_id=1, source_target_pairs={{0,4},{2,6},{4,0},{6,2},{8,12},{10,14},{12,8},{14,10},{1,5},{3,7},... | collective-permute-start | bytes 417800 | tf_op jit(solution)/shard_map/ppermute | solution.py:226
  28.0 9.2 %collective-permute-start.5 = (bf16[256,512]{1,0:T(8,128)(2,1)S(1)}, bf16[256,512]{1,0:T(8,128)(2,1)S(1)}, u32[]{:S(2)}, u32[]{:S(2)}) collective-permute-start(bf16[256,512]{1,0:T(8,128)(2,1)S(1)} %pad_maximum_fusion.2.refs_3_), channel_id=1, source_target_pairs={{0,2},{2,0},{4,6},{6,4},{8,10},{10,8},{12,14},{14,12},{1,3},{3,1},... | collective-permute-start | bytes 786440 | tf_op jit(solution)/shard_map/ppermute | solution.py:226
  29.5 9.2 %collective-permute-start.4 = (bf16[256,512]{1,0:T(8,128)(2,1)S(1)}, bf16[256,512]{1,0:T(8,128)(2,1)}, u32[]{:S(2)}, u32[]{:S(2)}) collective-permute-start(bf16[256,512]{1,0:T(8,128)(2,1)S(1)} %collective-permute-done.3.refs_5_), channel_id=1, source_target_pairs={{0,4},{2,6},{4,0},{6,2},{8,12},{10,14},{12,8},{14,10},{1,5},{3,7},... | collective-permute-start | bytes 786440 | tf_op jit(solution)/shard_map/ppermute | solution.py:226
  30.0 25.6 %collective-permute-start.1 = (bf16[128,2048]{1,0:T(8,128)(2,1)S(1)}, bf16[128,2048]{1,0:T(8,128)(2,1)S(1)}, u32[]{:S(2)}, u32[]{:S(2)}) collective-permute-start(bf16[128,2048]{1,0:T(8,128)(2,1)S(1)} %collective-permute-done.refs_1_), channel_id=1, source_target_pairs={{0,1},{1,0},{2,3},{3,2},{4,5},{5,4},{6,7},{7,6},{8,9},{9,8},{10,11... | collective-permute-start | bytes 1572872 | tf_op jit(solution)/shard_map/ppermute | solution.py:197
  30.0 12.7 %collective-permute-start.7 = (bf16[256,512]{1,0:T(8,128)(2,1)S(1)}, bf16[256,512]{1,0:T(8,128)(2,1)S(1)}, u32[]{:S(2)}, u32[]{:S(2)}) collective-permute-start(bf16[256,512]{1,0:T(8,128)(2,1)S(1)} %collective-permute-done.3.refs_5_), channel_id=1, source_target_pairs={{0,2},{2,0},{4,6},{6,4},{8,10},{10,8},{12,14},{14,12},{1,3},{3,1},... | collective-permute-start | bytes 786440 | tf_op jit(solution)/shard_map/ppermute | solution.py:226
  30.6 8.8 %collective-permute-start.14 = (bf16[272,256]{1,0:T(8,128)(2,1)}, bf16[272,256]{1,0:T(8,128)(2,1)S(1)}, u32[]{:S(2)}, u32[]{:S(2)}) collective-permute-start(bf16[272,256]{1,0:T(8,128)(2,1)} %collective-permute-done.13.refs_6_), channel_id=1, source_target_pairs={{0,4},{2,6},{4,0},{6,2},{8,12},{10,14},{12,8},{14,10},{1,5},{3,7},... | collective-permute-start | bytes 417800 | tf_op jit(solution)/shard_map/ppermute | solution.py:226
  37.1 11.3 %collective-permute-start.6 = (bf16[256,512]{1,0:T(8,128)(2,1)S(1)}, bf16[256,512]{1,0:T(8,128)(2,1)}, u32[]{:S(2)}, u32[]{:S(2)}) collective-permute-start(bf16[256,512]{1,0:T(8,128)(2,1)S(1)} %collective-permute-done.2.refs_4_), channel_id=1, source_target_pairs={{0,2},{2,0},{4,6},{6,4},{8,10},{10,8},{12,14},{14,12},{1,3},{3,1},... | collective-permute-start | bytes 786440 | tf_op jit(solution)/shard_map/ppermute | solution.py:226
  38.7 15.4 %collective-permute-start.8 = (bf16[256,512]{1,0:T(8,128)(2,1)}, bf16[256,512]{1,0:T(8,128)(2,1)}, u32[]{:S(2)}, u32[]{:S(2)}) collective-permute-start(bf16[256,512]{1,0:T(8,128)(2,1)} %collective-permute-done.4.refs_6_), channel_id=1, source_target_pairs={{0,2},{2,0},{4,6},{6,4},{8,10},{10,8},{12,14},{14,12},{1,3},{3,1},... | collective-permute-start | bytes 786440 | tf_op jit(solution)/shard_map/ppermute | solution.py:226
  39.4 25.3 %collective-permute-start.15 = (bf16[272,256]{1,0:T(8,128)(2,1)S(1)}, bf16[272,256]{1,0:T(8,128)(2,1)}, u32[]{:S(2)}, u32[]{:S(2)}) collective-permute-start(bf16[272,256]{1,0:T(8,128)(2,1)S(1)} %pad_maximum_fusion.3.refs_4_), channel_id=1, source_target_pairs={{0,2},{2,0},{4,6},{6,4},{8,10},{10,8},{12,14},{14,12},{1,3},{3,1},... | collective-permute-start | bytes 417800 | tf_op jit(solution)/shard_map/ppermute | solution.py:226
  43.5 21.2 %collective-permute-start.17 = (bf16[272,256]{1,0:T(8,128)(2,1)}, bf16[272,256]{1,0:T(8,128)(2,1)}, u32[]{:S(2)}, u32[]{:S(2)}) collective-permute-start(bf16[272,256]{1,0:T(8,128)(2,1)} %collective-permute-done.13.refs_6_), channel_id=1, source_target_pairs={{0,2},{2,0},{4,6},{6,4},{8,10},{10,8},{12,14},{14,12},{1,3},{3,1},... | collective-permute-start | bytes 417800 | tf_op jit(solution)/shard_map/ppermute | solution.py:226
  48.5 19.6 %collective-permute-start.16 = (bf16[272,256]{1,0:T(8,128)(2,1)}, bf16[272,256]{1,0:T(8,128)(2,1)}, u32[]{:S(2)}, u32[]{:S(2)}) collective-permute-start(bf16[272,256]{1,0:T(8,128)(2,1)} %collective-permute-done.12.refs_5_), channel_id=1, source_target_pairs={{0,2},{2,0},{4,6},{6,4},{8,10},{10,8},{12,14},{14,12},{1,3},{3,1},... | collective-permute-start | bytes 417800 | tf_op jit(solution)/shard_map/ppermute | solution.py:226
  54.1 14.6 %collective-permute-start.18 = (bf16[272,256]{1,0:T(8,128)(2,1)}, bf16[272,256]{1,0:T(8,128)(2,1)}, u32[]{:S(2)}, u32[]{:S(2)}) collective-permute-start(bf16[272,256]{1,0:T(8,128)(2,1)} %copy-done.50), channel_id=1, source_target_pairs={{0,2},{2,0},{4,6},{6,4},{8,10},{10,8},{12,14},{14,12},{1,3},{3,1},... | collective-permute-start | bytes 417800 | tf_op jit(solution)/shard_map/ppermute | solution.py:226
  64.2 4.5 %collective-permute-start.10 = (f32[8,512]{1,0:T(8,128)}, f32[8,512]{1,0:T(8,128)S(1)}, u32[]{:S(2)}, u32[]{:S(2)}) collective-permute-start(f32[8,512]{1,0:T(8,128)} %get-tuple-element.16.refs_0_), channel_id=1, source_target_pairs={{0,16},{1,17},{16,0},{17,1},{2,18},{3,19},{18,2},{19,3},{4,20},{5,... | collective-permute-start | bytes 49160 | tf_op jit(solution)/shard_map/ppermute | solution.py:358
  64.7 4.0 %collective-permute-start.11 = (f32[8,512]{1,0:T(8,128)}, f32[8,512]{1,0:T(8,128)S(1)}, u32[]{:S(2)}, u32[]{:S(2)}) collective-permute-start(f32[8,512]{1,0:T(8,128)} %get-tuple-element.16.refs_0_), channel_id=1, source_target_pairs={{0,17},{1,16},{16,1},{17,0},{2,19},{3,18},{18,3},{19,2},{4,21},{5,... | collective-permute-start | bytes 49160 | tf_op jit(solution)/shard_map/ppermute | solution.py:358
  64.7 4.0 %collective-permute-start.9 = (f32[8,512]{1,0:T(8,128)}, f32[8,512]{1,0:T(8,128)S(1)}, u32[]{:S(2)}, u32[]{:S(2)}) collective-permute-start(f32[8,512]{1,0:T(8,128)} %get-tuple-element.16.refs_0_), channel_id=1, source_target_pairs={{0,1},{1,0},{16,17},{17,16},{2,3},{3,2},{18,19},{19,18},{4,5},{5,4... | collective-permute-start | bytes 49160 | tf_op jit(solution)/shard_map/ppermute | solution.py:358
  68.1 18.0 %collective-permute-start.25 = (bf16[256,1024]{1,0:T(8,128)(2,1)S(1)}, bf16[256,1024]{1,0:T(8,128)(2,1)S(1)}, u32[]{:S(2)}, u32[]{:S(2)}) collective-permute-start(bf16[256,1024]{1,0:T(8,128)(2,1)S(1)} %get-tuple-element.29), channel_id=1, source_target_pairs={{0,4},{2,6},{4,0},{6,2},{8,12},{10,14},{12,8},{14,10},{1,5},{3,7},... | collective-permute-start | bytes 1572872 | tf_op jit(solution)/shard_map/ppermute | solution.py:226
  74.0 76.8 %collective-permute-start.19 = (bf16[256,2048]{1,0:T(8,128)(2,1)}, bf16[256,2048]{1,0:T(8,128)(2,1)S(1)}, u32[]{:S(2)}, u32[]{:S(2)}) collective-permute-start(bf16[256,2048]{1,0:T(8,128)(2,1)} %get-tuple-element.18), channel_id=1, source_target_pairs={{0,1},{1,0},{2,3},{3,2},{4,5},{5,4},{6,7},{7,6},{8,9},{9,8},{10,11... | collective-permute-start | bytes 3145736 | tf_op jit(solution)/shard_map/ppermute | solution.py:197
  74.8 4.4 %collective-permute-start.21 = (f32[1,1024]{1,0:T(1,128)S(1)}, f32[1,1024]{1,0:T(1,128)S(1)}, u32[]{:S(2)}, u32[]{:S(2)}) collective-permute-start(f32[1,1024]{1,0:T(1,128)S(1)} %bitcast.8), channel_id=1, source_target_pairs={{0,1},{1,0},{2,3},{3,2},{4,5},{5,4},{6,7},{7,6},{8,9},{9,8},{10,11... | collective-permute-start | bytes 12296 | tf_op jit(solution)/shard_map/ppermute | solution.py:197
  75.3 38.8 %collective-permute-start.26 = (bf16[256,1024]{1,0:T(8,128)(2,1)S(1)}, bf16[256,1024]{1,0:T(8,128)(2,1)S(1)}, u32[]{:S(2)}, u32[]{:S(2)}) collective-permute-start(bf16[256,1024]{1,0:T(8,128)(2,1)S(1)} %get-tuple-element.30.refs_6_), channel_id=1, source_target_pairs={{0,8},{2,10},{4,12},{6,14},{8,0},{10,2},{12,4},{14,6},{1,9},{3,11}... | collective-permute-start | bytes 1572872 | tf_op jit(solution)/shard_map/ppermute | solution.py:226
  78.9 35.3 %collective-permute-start.27 = (bf16[256,1024]{1,0:T(8,128)(2,1)S(1)}, bf16[256,1024]{1,0:T(8,128)(2,1)S(1)}, u32[]{:S(2)}, u32[]{:S(2)}) collective-permute-start(bf16[256,1024]{1,0:T(8,128)(2,1)S(1)} %get-tuple-element.29), channel_id=1, source_target_pairs={{0,12},{2,14},{4,8},{6,10},{8,4},{10,6},{12,0},{14,2},{1,13},{3,15... | collective-permute-start | bytes 1572872 | tf_op jit(solution)/shard_map/ppermute | solution.py:226
  79.2 37.5 %collective-permute-start.28 = (bf16[256,1024]{1,0:T(8,128)(2,1)S(1)}, bf16[256,1024]{1,0:T(8,128)(2,1)S(1)}, u32[]{:S(2)}, u32[]{:S(2)}) collective-permute-start(bf16[256,1024]{1,0:T(8,128)(2,1)S(1)} %get-tuple-element.30.refs_6_), channel_id=1, source_target_pairs={{0,2},{2,0},{4,6},{6,4},{8,10},{10,8},{12,14},{14,12},{1,3},{3,1},... | collective-permute-start | bytes 1572872 | tf_op jit(solution)/shard_map/ppermute | solution.py:226
  86.1 64.3 %collective-permute-start.32 = (bf16[256,1024]{1,0:T(8,128)(2,1)S(1)}, bf16[256,1024]{1,0:T(8,128)(2,1)}, u32[]{:S(2)}, u32[]{:S(2)}) collective-permute-start(bf16[256,1024]{1,0:T(8,128)(2,1)S(1)} %get-tuple-element.30.refs_6_), channel_id=1, source_target_pairs={{0,1},{1,0},{2,3},{3,2},{4,5},{5,4},{6,7},{7,6},{8,9},{9,8},{10,11... | collective-permute-start | bytes 1572872 | tf_op jit(solution)/shard_map/ppermute | solution.py:197
  114.2 45.5 %collective-permute-start.49 = (bf16[1040,256]{1,0:T(8,128)(2,1)S(1)}, bf16[1040,256]{1,0:T(8,128)(2,1)S(1)}, u32[]{:S(2)}, u32[]{:S(2)}) collective-permute-start(bf16[1040,256]{1,0:T(8,128)(2,1)S(1)} %get-tuple-element.36.refs_0_), channel_id=1, source_target_pairs={{0,8},{2,10},{4,12},{6,14},{8,0},{10,2},{12,4},{14,6},{1,9},{3,11}... | collective-permute-start | bytes 1597448 | tf_op jit(solution)/shard_map/ppermute | solution.py:226
  114.2 46.0 %collective-permute-start.50 = (bf16[1040,256]{1,0:T(8,128)(2,1)S(1)}, bf16[1040,256]{1,0:T(8,128)(2,1)S(1)}, u32[]{:S(2)}, u32[]{:S(2)}) collective-permute-start(bf16[1040,256]{1,0:T(8,128)(2,1)S(1)} %get-tuple-element.35), channel_id=1, source_target_pairs={{0,12},{2,14},{4,8},{6,10},{8,4},{10,6},{12,0},{14,2},{1,13},{3,15... | collective-permute-start | bytes 1597448 | tf_op jit(solution)/shard_map/ppermute | solution.py:226
  116.7 53.6 %collective-permute-start.40 = (bf16[1040,256]{1,0:T(8,128)(2,1)S(1)}, bf16[1040,256]{1,0:T(8,128)(2,1)S(1)}, u32[]{:S(2)}, u32[]{:S(2)}) collective-permute-start(bf16[1040,256]{1,0:T(8,128)(2,1)S(1)} %get-tuple-element.35), channel_id=1, source_target_pairs={{0,4},{2,6},{4,0},{6,2},{8,12},{10,14},{12,8},{14,10},{1,5},{3,7},... | collective-permute-start | bytes 1597448 | tf_op jit(solution)/shard_map/ppermute | solution.py:226
  150.4 20.4 %collective-permute-start.41 = (bf16[1040,256]{1,0:T(8,128)(2,1)S(1)}, bf16[1040,256]{1,0:T(8,128)(2,1)S(1)}, u32[]{:S(2)}, u32[]{:S(2)}) collective-permute-start(bf16[1040,256]{1,0:T(8,128)(2,1)S(1)} %get-tuple-element.36.refs_0_), channel_id=1, source_target_pairs={{0,2},{2,0},{4,6},{6,4},{8,10},{10,8},{12,14},{14,12},{1,3},{3,1},... | collective-permute-start | bytes 1597448 | tf_op jit(solution)/shard_map/ppermute | solution.py:226
  150.9 20.4 %collective-permute-start.43 = (bf16[1040,256]{1,0:T(8,128)(2,1)S(1)}, bf16[1040,256]{1,0:T(8,128)(2,1)S(1)}, u32[]{:S(2)}, u32[]{:S(2)}) collective-permute-start(bf16[1040,256]{1,0:T(8,128)(2,1)S(1)} %get-tuple-element.36.refs_0_), channel_id=1, source_target_pairs={{0,1},{1,0},{2,3},{3,2},{4,5},{5,4},{6,7},{7,6},{8,9},{9,8},{10,11... | collective-permute-start | bytes 1597448 | tf_op jit(solution)/shard_map/ppermute | solution.py:197
  159.7 14.8 %collective-permute-start.29 = (bf16[256,1024]{1,0:T(8,128)(2,1)S(1)}, bf16[256,1024]{1,0:T(8,128)(2,1)S(1)}, u32[]{:S(2)}, u32[]{:S(2)}) collective-permute-start(bf16[256,1024]{1,0:T(8,128)(2,1)S(1)} %copy-done.20), channel_id=1, source_target_pairs={{0,2},{2,0},{4,6},{6,4},{8,10},{10,8},{12,14},{14,12},{1,3},{3,1},... | collective-permute-start | bytes 1572872 | tf_op jit(solution)/shard_map/ppermute | solution.py:226
  160.2 25.5 %collective-permute-start.30 = (bf16[256,1024]{1,0:T(8,128)(2,1)S(1)}, bf16[256,1024]{1,0:T(8,128)(2,1)S(1)}, u32[]{:S(2)}, u32[]{:S(2)}) collective-permute-start(bf16[256,1024]{1,0:T(8,128)(2,1)S(1)} %collective-permute-done.26.refs_8_), channel_id=1, source_target_pairs={{0,2},{2,0},{4,6},{6,4},{8,10},{10,8},{12,14},{14,12},{1,3},{3,1},... | collective-permute-start | bytes 1572872 | tf_op jit(solution)/shard_map/ppermute | solution.py:226
  170.4 15.3 %collective-permute-start.20 = (bf16[128,2048]{1,0:T(8,128)(2,1)S(1)}, bf16[128,2048]{1,0:T(8,128)(2,1)S(1)}, u32[]{:S(2)}, u32[]{:S(2)}) collective-permute-start(bf16[128,2048]{1,0:T(8,128)(2,1)S(1)} %add_convert_fusion.1), channel_id=1, source_target_pairs={{0,16},{16,0},{1,17},{17,1},{2,18},{18,2},{3,19},{19,3},{4,20},{20... | collective-permute-start | bytes 1572872 | tf_op jit(solution)/shard_map/ppermute | solution.py:197
  170.8 24.9 %collective-permute-start.31 = (bf16[256,1024]{1,0:T(8,128)(2,1)S(1)}, bf16[256,1024]{1,0:T(8,128)(2,1)S(1)}, u32[]{:S(2)}, u32[]{:S(2)}) collective-permute-start(bf16[256,1024]{1,0:T(8,128)(2,1)S(1)} %collective-permute-done.27.refs_9_), channel_id=1, source_target_pairs={{0,2},{2,0},{4,6},{6,4},{8,10},{10,8},{12,14},{14,12},{1,3},{3,1},... | collective-permute-start | bytes 1572872 | tf_op jit(solution)/shard_map/ppermute | solution.py:226
  171.3 25.0 %collective-permute-start.33 = (bf16[256,1024]{1,0:T(8,128)(2,1)S(1)}, bf16[256,1024]{1,0:T(8,128)(2,1)S(1)}, u32[]{:S(2)}, u32[]{:S(2)}) collective-permute-start(bf16[256,1024]{1,0:T(8,128)(2,1)S(1)} %copy-done.20), channel_id=1, source_target_pairs={{0,1},{1,0},{2,3},{3,2},{4,5},{5,4},{6,7},{7,6},{8,9},{9,8},{10,11... | collective-permute-start | bytes 1572872 | tf_op jit(solution)/shard_map/ppermute | solution.py:197
  174.5 23.4 %collective-permute-start.34 = (bf16[256,1024]{1,0:T(8,128)(2,1)S(1)}, bf16[256,1024]{1,0:T(8,128)(2,1)S(1)}, u32[]{:S(2)}, u32[]{:S(2)}) collective-permute-start(bf16[256,1024]{1,0:T(8,128)(2,1)S(1)} %collective-permute-done.26.refs_8_), channel_id=1, source_target_pairs={{0,1},{1,0},{2,3},{3,2},{4,5},{5,4},{6,7},{7,6},{8,9},{9,8},{10,11... | collective-permute-start | bytes 1572872 | tf_op jit(solution)/shard_map/ppermute | solution.py:197
  185.7 12.2 %collective-permute-start.35 = (bf16[256,1024]{1,0:T(8,128)(2,1)S(1)}, bf16[256,1024]{1,0:T(8,128)(2,1)S(1)}, u32[]{:S(2)}, u32[]{:S(2)}) collective-permute-start(bf16[256,1024]{1,0:T(8,128)(2,1)S(1)} %collective-permute-done.27.refs_9_), channel_id=1, source_target_pairs={{0,1},{1,0},{2,3},{3,2},{4,5},{5,4},{6,7},{7,6},{8,9},{9,8},{10,11... | collective-permute-start | bytes 1572872 | tf_op jit(solution)/shard_map/ppermute | solution.py:197
  185.7 12.8 %collective-permute-start.36 = (bf16[256,1024]{1,0:T(8,128)(2,1)S(1)}, bf16[256,1024]{1,0:T(8,128)(2,1)S(1)}, u32[]{:S(2)}, u32[]{:S(2)}) collective-permute-start(bf16[256,1024]{1,0:T(8,128)(2,1)S(1)} %collective-permute-done.28.refs_10_), channel_id=1, source_target_pairs={{0,1},{1,0},{2,3},{3,2},{4,5},{5,4},{6,7},{7,6},{8,9},{9,8},{10,11... | collective-permute-start | bytes 1572872 | tf_op jit(solution)/shard_map/ppermute | solution.py:197
  195.8 15.0 %collective-permute-start.55 = (bf16[1040,256]{1,0:T(8,128)(2,1)S(1)}, bf16[1040,256]{1,0:T(8,128)(2,1)S(1)}, u32[]{:S(2)}, u32[]{:S(2)}) collective-permute-start(bf16[1040,256]{1,0:T(8,128)(2,1)S(1)} %collective-permute-done.49.refs_0_), channel_id=1, source_target_pairs={{0,2},{2,0},{4,6},{6,4},{8,10},{10,8},{12,14},{14,12},{1,3},{3,1},... | collective-permute-start | bytes 1597448 | tf_op jit(solution)/shard_map/ppermute | solution.py:226
  196.3 35.4 %collective-permute-start.42 = (bf16[1040,256]{1,0:T(8,128)(2,1)S(1)}, bf16[1040,256]{1,0:T(8,128)(2,1)}, u32[]{:S(2)}, u32[]{:S(2)}) collective-permute-start(bf16[1040,256]{1,0:T(8,128)(2,1)S(1)} %collective-permute-done.40.refs_1_), channel_id=1, source_target_pairs={{0,2},{2,0},{4,6},{6,4},{8,10},{10,8},{12,14},{14,12},{1,3},{3,1},... | collective-permute-start | bytes 1597448 | tf_op jit(solution)/shard_map/ppermute | solution.py:226
  197.9 34.3 %collective-permute-start.44 = (bf16[1040,256]{1,0:T(8,128)(2,1)S(1)}, bf16[1040,256]{1,0:T(8,128)(2,1)S(1)}, u32[]{:S(2)}, u32[]{:S(2)}) collective-permute-start(bf16[1040,256]{1,0:T(8,128)(2,1)S(1)} %collective-permute-done.40.refs_1_), channel_id=1, source_target_pairs={{0,1},{1,0},{2,3},{3,2},{4,5},{5,4},{6,7},{7,6},{8,9},{9,8},{10,11... | collective-permute-start | bytes 1597448 | tf_op jit(solution)/shard_map/ppermute | solution.py:197
  197.9 33.7 %collective-permute-start.56 = (bf16[1040,256]{1,0:T(8,128)(2,1)S(1)}, bf16[1040,256]{1,0:T(8,128)(2,1)}, u32[]{:S(2)}, u32[]{:S(2)}) collective-permute-start(bf16[1040,256]{1,0:T(8,128)(2,1)S(1)} %collective-permute-done.50.refs_1_), channel_id=1, source_target_pairs={{0,2},{2,0},{4,6},{6,4},{8,10},{10,8},{12,14},{14,12},{1,3},{3,1},... | collective-permute-start | bytes 1597448 | tf_op jit(solution)/shard_map/ppermute | solution.py:226
  198.5 33.8 %collective-permute-start.45 = (bf16[1040,256]{1,0:T(8,128)(2,1)S(1)}, bf16[1040,256]{1,0:T(8,128)(2,1)S(1)}, u32[]{:S(2)}, u32[]{:S(2)}) collective-permute-start(bf16[1040,256]{1,0:T(8,128)(2,1)S(1)} %collective-permute-done.41.refs_2_), channel_id=1, source_target_pairs={{0,1},{1,0},{2,3},{3,2},{4,5},{5,4},{6,7},{7,6},{8,9},{9,8},{10,11... | collective-permute-start | bytes 1597448 | tf_op jit(solution)/shard_map/ppermute | solution.py:197
  210.7 22.1 %collective-permute-start.23 = (bf16[128,2048]{1,0:T(8,128)(2,1)S(1)}, bf16[128,2048]{1,0:T(8,128)(2,1)S(1)}, u32[]{:S(2)}, u32[]{:S(2)}) collective-permute-start(bf16[128,2048]{1,0:T(8,128)(2,1)S(1)} %fusion.5.refs_2_), channel_id=1, source_target_pairs={{0,4},{2,6},{4,0},{6,2},{8,12},{10,14},{12,8},{14,10},{1,5},{3,7},... | collective-permute-start | bytes 1572872 | tf_op jit(solution)/shard_map/ppermute | solution.py:226
  231.6 2.6 collective-permute-start.37
  231.6 2.7 collective-permute-start.38
  232.1 2.9 collective-permute-start.39
  232.2 14.8 %collective-permute-start.22 = (bf16[128,2048]{1,0:T(8,128)(2,1)S(1)}, bf16[128,2048]{1,0:T(8,128)(2,1)S(1)}, u32[]{:S(2)}, u32[]{:S(2)}) collective-permute-start(bf16[128,2048]{1,0:T(8,128)(2,1)S(1)} %fusion.5.refs_2_), channel_id=1, source_target_pairs={{0,16},{16,0},{1,17},{17,1},{2,18},{18,2},{3,19},{19,3},{4,20},{20... | collective-permute-start | bytes 1572872 | tf_op jit(solution)/shard_map/ppermute | solution.py:197
  232.8 24.9 %collective-permute-start.24 = (bf16[128,2048]{1,0:T(8,128)(2,1)S(1)}, bf16[128,2048]{1,0:T(8,128)(2,1)S(1)}, u32[]{:S(2)}, u32[]{:S(2)}) collective-permute-start(bf16[128,2048]{1,0:T(8,128)(2,1)S(1)} %collective-permute-done.23.refs_4_), channel_id=1, source_target_pairs={{0,16},{16,0},{1,17},{17,1},{2,18},{18,2},{3,19},{19,3},{4,20},{20... | collective-permute-start | bytes 1572872 | tf_op jit(solution)/shard_map/ppermute | solution.py:197
  234.3 34.1 %collective-permute-start.46 = (bf16[1040,256]{1,0:T(8,128)(2,1)}, bf16[1040,256]{1,0:T(8,128)(2,1)}, u32[]{:S(2)}, u32[]{:S(2)}) collective-permute-start(bf16[1040,256]{1,0:T(8,128)(2,1)} %collective-permute-done.42.refs_3_), channel_id=1, source_target_pairs={{0,1},{1,0},{2,3},{3,2},{4,5},{5,4},{6,7},{7,6},{8,9},{9,8},{10,11... | collective-permute-start | bytes 1597448 | tf_op jit(solution)/shard_map/ppermute | solution.py:197
  234.3 41.8 %collective-permute-start.57 = (bf16[1040,256]{1,0:T(8,128)(2,1)S(1)}, bf16[1040,256]{1,0:T(8,128)(2,1)}, u32[]{:S(2)}, u32[]{:S(2)}) collective-permute-start(bf16[1040,256]{1,0:T(8,128)(2,1)S(1)} %collective-permute-done.55.refs_0_), channel_id=1, source_target_pairs={{0,1},{1,0},{2,3},{3,2},{4,5},{5,4},{6,7},{7,6},{8,9},{9,8},{10,11... | collective-permute-start | bytes 1597448 | tf_op jit(solution)/shard_map/ppermute | solution.py:197
  235.0 41.1 %collective-permute-start.58 = (bf16[1040,256]{1,0:T(8,128)(2,1)}, bf16[1040,256]{1,0:T(8,128)(2,1)}, u32[]{:S(2)}, u32[]{:S(2)}) collective-permute-start(bf16[1040,256]{1,0:T(8,128)(2,1)} %collective-permute-done.56.refs_1_), channel_id=1, source_target_pairs={{0,1},{1,0},{2,3},{3,2},{4,5},{5,4},{6,7},{7,6},{8,9},{9,8},{10,11... | collective-permute-start | bytes 1597448 | tf_op jit(solution)/shard_map/ppermute | solution.py:197
  247.0 36.2 %collective-permute-start.51 = (bf16[1040,256]{1,0:T(8,128)(2,1)S(1)}, bf16[1040,256]{1,0:T(8,128)(2,1)}, u32[]{:S(2)}, u32[]{:S(2)}) collective-permute-start(bf16[1040,256]{1,0:T(8,128)(2,1)S(1)} %collective-permute-done.49.refs_0_), channel_id=1, source_target_pairs={{0,1},{1,0},{2,3},{3,2},{4,5},{5,4},{6,7},{7,6},{8,9},{9,8},{10,11... | collective-permute-start | bytes 1597448 | tf_op jit(solution)/shard_map/ppermute | solution.py:197
  258.7 24.6 %collective-permute-start.52 = (bf16[1040,256]{1,0:T(8,128)(2,1)S(1)}, bf16[1040,256]{1,0:T(8,128)(2,1)}, u32[]{:S(2)}, u32[]{:S(2)}) collective-permute-start(bf16[1040,256]{1,0:T(8,128)(2,1)S(1)} %collective-permute-done.50.refs_1_), channel_id=1, source_target_pairs={{0,1},{1,0},{2,3},{3,2},{4,5},{5,4},{6,7},{7,6},{8,9},{9,8},{10,11... | collective-permute-start | bytes 1597448 | tf_op jit(solution)/shard_map/ppermute | solution.py:197
  275.5 21.0 %collective-permute-start.47 = (bf16[256,1024]{1,0:T(8,128)(2,1)}, bf16[256,1024]{1,0:T(8,128)(2,1)}, u32[]{:S(2)}, u32[]{:S(2)}) collective-permute-start(bf16[256,1024]{1,0:T(8,128)(2,1)} %get-tuple-element.20), channel_id=1, source_target_pairs={{0,16},{16,0},{1,17},{17,1},{2,18},{18,2},{3,19},{19,3},{4,20},{20... | collective-permute-start | bytes 1572872 | tf_op jit(solution)/shard_map/ppermute | solution.py:197
  281.1 14.6 %collective-permute-start.59 = (bf16[256,512]{1,0:T(8,128)(2,1)}, bf16[256,512]{1,0:T(8,128)(2,1)S(1)}, u32[]{:S(2)}, u32[]{:S(2)}) collective-permute-start(bf16[256,512]{1,0:T(8,128)(2,1)} %get-tuple-element.24), channel_id=1, source_target_pairs={{0,16},{16,0},{1,17},{17,1},{2,18},{18,2},{3,19},{19,3},{4,20},{20... | collective-permute-start | bytes 786440 | tf_op jit(solution)/shard_map/ppermute | solution.py:197
  288.5 10.4 %collective-permute-start.53 = (bf16[256,512]{1,0:T(8,128)(2,1)}, bf16[256,512]{1,0:T(8,128)(2,1)S(1)}, u32[]{:S(2)}, u32[]{:S(2)}) collective-permute-start(bf16[256,512]{1,0:T(8,128)(2,1)} %get-tuple-element.22), channel_id=1, source_target_pairs={{0,4},{2,6},{4,0},{6,2},{8,12},{10,14},{12,8},{14,10},{1,5},{3,7},... | collective-permute-start | bytes 786440 | tf_op jit(solution)/shard_map/ppermute | solution.py:226
  295.7 6.4 %collective-permute-start.60 = (bf16[128,512]{1,0:T(8,128)(2,1)S(1)}, bf16[128,512]{1,0:T(8,128)(2,1)S(1)}, u32[]{:S(2)}, u32[]{:S(2)}) collective-permute-start(bf16[128,512]{1,0:T(8,128)(2,1)S(1)} %add_convert_fusion.5), channel_id=1, source_target_pairs={{0,4},{2,6},{4,0},{6,2},{8,12},{10,14},{12,8},{14,10},{1,5},{3,7},... | collective-permute-start | bytes 393224 | tf_op jit(solution)/shard_map/ppermute | solution.py:226
  297.4 9.0 %collective-permute-start.48 = (bf16[128,1024]{1,0:T(8,128)(2,1)S(1)}, bf16[128,1024]{1,0:T(8,128)(2,1)S(1)}, u32[]{:S(2)}, u32[]{:S(2)}) collective-permute-start(bf16[128,1024]{1,0:T(8,128)(2,1)S(1)} %add_convert_fusion.3), channel_id=1, source_target_pairs={{0,4},{2,6},{4,0},{6,2},{8,12},{10,14},{12,8},{14,10},{1,5},{3,7},... | collective-permute-start | bytes 786440 | tf_op jit(solution)/shard_map/ppermute | solution.py:226
  299.9 7.7 %collective-permute-start.54 = (bf16[128,512]{1,0:T(8,128)(2,1)S(1)}, bf16[128,512]{1,0:T(8,128)(2,1)S(1)}, u32[]{:S(2)}, u32[]{:S(2)}) collective-permute-start(bf16[128,512]{1,0:T(8,128)(2,1)S(1)} %add_convert_fusion.7), channel_id=1, source_target_pairs={{0,16},{16,0},{1,17},{17,1},{2,18},{18,2},{3,19},{19,3},{4,20},{20... | collective-permute-start | bytes 393224 | tf_op jit(solution)/shard_map/ppermute | solution.py:197
  302.2 6.0 %collective-permute-start.63 = (bf16[128,512]{1,0:T(8,128)(2,1)S(1)}, bf16[128,512]{1,0:T(8,128)(2,1)S(1)}, u32[]{:S(2)}, u32[]{:S(2)}) collective-permute-start(bf16[128,512]{1,0:T(8,128)(2,1)S(1)} %add_convert_fusion.4.refs_2_), channel_id=1, source_target_pairs={{0,1},{1,0},{2,3},{3,2},{4,5},{5,4},{6,7},{7,6},{8,9},{9,8},{10,11... | collective-permute-start | bytes 393224 | tf_op jit(solution)/shard_map/ppermute | solution.py:197
  307.5 1.8 collective-permute-start.61
  307.7 1.6 collective-permute-start.62
  (61 other events, 2611.8 us)
